TPU v7x, 256 devices: a whole 4x4x8 slice. The times are simulated.
256 devices in a mesh: ep: 64 (over z, x, core), tp: 4 (over y).
Axes of the slice: x: 4, y: 4, z: 8, core: 2. Of those that a mesh axis runs over, the one named last changes fastest.
Arguments:
- tokens: bfloat16 [16384, 2048], P('ep'), may hold values from -6 to 6
- routes: int32 [16384, 4], P('ep'), may hold values from 0 to 63, all different within a row; in each aligned block of 256 rows (0 to 255, 256 to 511, ...) at most 20 rows name the same one
- gate_weights: float32 [16384, 4], P('ep'), may hold values from 0.05 to 1
- out_grad: bfloat16 [16384, 2048], P('ep'), may hold values from -0.59765625 to 0.59765625
- w_gate: bfloat16 [64, 2048, 1024], P('ep', None, 'tp'), may hold values from -0.1875 to 0.1875
- w_up: bfloat16 [64, 2048, 1024], P('ep', None, 'tp'), may hold values from -0.1875 to 0.1875
- w_down: bfloat16 [64, 1024, 2048], P('ep', 'tp'), may hold values from -0.1875 to 0.1875
Outputs:
- token_grad: bfloat16 [16384, 2048], P('ep', 'tp')
- gate_grad: float32 [16384, 4], P('ep')
- gate_weight_grad: float32 [64, 2048, 1024], P('ep', None, 'tp')
- up_weight_grad: float32 [64, 2048, 1024], P('ep', None, 'tp')
- down_weight_grad: float32 [64, 1024, 2048], P('ep', 'tp')
Inputs may be any that keep to these rules, and one draw needn't show every extreme that they name: `routes`: each row names 4 different experts. In each aligned block of 256 rows (the rows of one device) no expert is named by more than 20 rows, and in some block an expert is named by exactly 20 rows.
All inputs are finite; a program needn't handle non-finite values.
Results may differ from a plain program's by a relative error of at most 0.012.
Values may be sent and summed in bfloat16 or wider, within the bound.
A program may use at most 128 MiB of HBM per device.

v0:
```python
import jax
import jax.numpy as jnp
from jax import lax
from jax.sharding import Mesh
from jax.sharding import PartitionSpec as P

EP = ("ep_0", "ep_1", "ep_2")


clamp_limit = 7.0
sigmoid_slope = 1.702


def in_one_piece(arrays, axis, split_dim, concat_dim, along):
    widths = [a.shape[along] for a in arrays]
    both = jnp.concatenate(arrays, axis=along)
    result = lax.all_to_all(both, axis, split_axis=split_dim, concat_axis=concat_dim, tiled=True)
    return tuple(jnp.split(result, [sum(widths[:k]) for k in range(1, len(widths))], axis=along))


def in_one_piece_2(arrays, axis, dim, along):
    both = jnp.concatenate(arrays, axis=along)
    result, at, outs = (lax.all_gather(both, axis, axis=dim, tiled=True), 0, [])
    for a in arrays:
        outs.append(lax.slice_in_dim(result, at, at + a.shape[along], axis=along))
        at += a.shape[along]
    return tuple(outs)


def sent_to_all(x, axis):
    copies = jnp.broadcast_to(x, (lax.axis_size(axis), *x.shape))
    return lax.all_to_all(copies, axis, split_axis=0, concat_axis=0, tiled=True)


def of_everyone(x, axis):
    everything = sent_to_all(x, axis)
    return jnp.sum(everything, axis=0)


def split_up(x, dim, size):
    before, after = (x.shape[:dim], x.shape[dim + 1 :])
    return jnp.moveaxis(x.reshape(*before, size, -1, *after), dim, 0)


def joined_along(pieces, dim):
    lengths = list(pieces.shape[1:])
    lengths[dim] *= pieces.shape[0]
    return jnp.moveaxis(pieces, 0, dim).reshape(lengths)


def moved_by_axis(pieces, axes, order):
    inside = pieces.shape[1:]
    result = pieces.reshape(*(lax.axis_size(a) for a in axes), *inside)
    for k in order:
        result = lax.all_to_all(result, axes[k], k, k, tiled=True)
    return result.reshape(-1, *inside)


def two_step_exchange(x, groups, order, split_dim, concat_dim):
    size = lax.axis_size(groups[0]) * lax.axis_size(groups[1])
    pieces = split_up(x, split_dim, size)
    return joined_along(moved_by_axis(pieces, groups, order), concat_dim)


def unit_backward(gate_pre, up_pre, hidden_grad):
    glu = jnp.minimum(gate_pre, clamp_limit)
    linear = jnp.clip(up_pre, -clamp_limit, clamp_limit)
    sigma = jax.nn.sigmoid(sigmoid_slope * glu)
    active = glu * sigma
    hidden = (active * (linear + 1.0)).astype(jnp.bfloat16)
    slope_term = sigma + sigmoid_slope * active * (1.0 - sigma)
    gate_pre_grad = jnp.where(
        gate_pre < clamp_limit, hidden_grad * (linear + 1.0) * slope_term, 0.0
    ).astype(jnp.bfloat16)
    up_pre_grad = jnp.where(jnp.abs(up_pre) < clamp_limit, hidden_grad * active, 0.0).astype(
        jnp.bfloat16
    )
    return (hidden, gate_pre_grad, up_pre_grad)


def local(tokens, routes, gate_weights, out_grad, w_gate, w_up, w_down):
    ep_count = lax.axis_size(EP)
    tp_count = lax.axis_size("tp")
    tp_index = lax.axis_index("tp")
    token_count, model_width = tokens.shape
    top_count = routes.shape[1]
    expert_local = w_gate.shape[0]
    experts_all = ep_count * expert_local
    capacity = token_count * top_count * 5 // (4 * experts_all)
    pair_count = token_count * top_count
    width_cols = model_width // tp_count
    flat_routes = routes.reshape(-1)
    onehot = (flat_routes[:, None] == jnp.arange(experts_all, dtype=jnp.int32)[None, :]).astype(
        jnp.int32
    )
    slot_rank = jnp.sum((jnp.cumsum(onehot, axis=0) - onehot) * onehot, axis=1)
    target = flat_routes * capacity + slot_rank
    pair_index = jnp.arange(pair_count, dtype=jnp.int32)
    pair_table = jnp.zeros((experts_all * capacity,), jnp.int32).at[target].set(pair_index)
    is_live = jnp.zeros((experts_all * capacity,), jnp.int32).at[target].set(1) > 0
    token_index = pair_table // top_count
    flat_weights = gate_weights.reshape(-1)
    live_column = is_live[:, None]
    send_rows = jnp.where(live_column, tokens[token_index], jnp.zeros((), jnp.bfloat16))
    send_grads = jnp.where(live_column, out_grad[token_index], jnp.zeros((), jnp.bfloat16))
    send_weights = jnp.where(is_live, flat_weights[pair_table], 0.0)
    col_start = tp_index * width_cols
    part_rows = lax.dynamic_slice_in_dim(send_rows, col_start, width_cols, 1)
    part_grads = lax.dynamic_slice_in_dim(send_grads, col_start, width_cols, 1)
    part_rows, part_grads = in_one_piece((part_rows, part_grads), EP, 0, 0, 1)
    arrived, arrived_grads = in_one_piece_2((part_rows, part_grads), "tp", 1, 0)
    arrived_weights = lax.all_to_all(send_weights, EP, split_axis=0, concat_axis=0, tiled=True)
    row_count = ep_count * capacity
    grouped_rows = arrived.reshape(ep_count, expert_local, capacity, model_width)
    grouped_grads = arrived_grads.reshape(ep_count, expert_local, capacity, model_width)
    grouped_weights = arrived_weights.reshape(ep_count, expert_local, capacity)
    gate_grads, up_grads, down_grads, row_terms, product_terms = ([], [], [], [], [])
    x_rows = grouped_rows[:, 0].reshape(row_count, model_width)
    dy_rows = grouped_grads[:, 0].reshape(row_count, model_width)
    slot_weights = grouped_weights[:, 0].reshape(row_count, 1)
    scaled = (slot_weights * dy_rows.astype(jnp.float32)).astype(jnp.bfloat16)
    gate_pre = jnp.dot(x_rows, w_gate[0], preferred_element_type=jnp.float32)
    up_pre = jnp.dot(x_rows, w_up[0], preferred_element_type=jnp.float32)
    hidden_grad = jnp.einsum("rd,fd->rf", scaled, w_down[0], preferred_element_type=jnp.float32)
    hidden, gate_pre_grad, up_pre_grad = unit_backward(gate_pre, up_pre, hidden_grad)
    gate_grads.append(
        jnp.einsum("rd,rf->df", x_rows, gate_pre_grad, preferred_element_type=jnp.float32)
    )
    up_grads.append(
        jnp.einsum("rd,rf->df", x_rows, up_pre_grad, preferred_element_type=jnp.float32)
    )
    down_grads.append(jnp.einsum("rf,rd->fd", hidden, scaled, preferred_element_type=jnp.float32))
    row_term = jnp.einsum("rf,df->rd", gate_pre_grad, w_gate[0], preferred_element_type=jnp.float32)
    row_term = row_term + jnp.einsum(
        "rf,df->rd", up_pre_grad, w_up[0], preferred_element_type=jnp.float32
    )
    row_terms.append(row_term.astype(jnp.bfloat16).reshape(ep_count, capacity, model_width))
    out_term = jnp.dot(hidden, w_down[0], preferred_element_type=jnp.float32).astype(jnp.bfloat16)
    product = jnp.sum(dy_rows.astype(jnp.float32) * out_term.astype(jnp.float32), axis=1)
    product_terms.append(product.reshape(ep_count, capacity))
    all_rows = jnp.stack(row_terms, axis=1).reshape(experts_all * capacity, model_width)
    all_products = jnp.stack(product_terms, axis=1).reshape(experts_all * capacity)
    row_sum = lax.psum_scatter(all_rows, "tp", scatter_dimension=1, tiled=True).astype(jnp.float32)
    product_sum = of_everyone(all_products, "tp")
    back_rows = lax.all_to_all(
        row_sum.astype(jnp.bfloat16), EP, split_axis=0, concat_axis=0, tiled=True
    )
    back_products = two_step_exchange(product_sum, (("ep_0", "ep_1"), "ep_2"), (1, 0), 0, 0)
    pair_rows = back_rows[target].reshape(token_count, top_count, width_cols)
    token_grad = jnp.sum(pair_rows.astype(jnp.float32), axis=1).astype(jnp.bfloat16)
    gate_grad = back_products[target].reshape(token_count, top_count)
    return (
        token_grad,
        gate_grad,
        jnp.stack(gate_grads),
        jnp.stack(up_grads),
        jnp.stack(down_grads),
    )


def solution(mesh):
    finer = Mesh(mesh.devices.reshape(8, 4, 2, mesh.shape["tp"]), ("ep_0", "ep_1", "ep_2", "tp"))
    in_specs = (
        P(EP, None),
        P(EP, None),
        P(EP, None),
        P(EP, None),
        P(EP, None, "tp"),
        P(EP, None, "tp"),
        P(EP, "tp", None),
    )
    out_specs = (P(EP, "tp"), P(EP, None), P(EP, None, "tp"), P(EP, None, "tp"), P(EP, "tp", None))
    return jax.shard_map(local, mesh=finer, in_specs=in_specs, out_specs=out_specs, check_vma=False)
```

profile of v0, /device:TPU:1, one launch (start us, length us, event | category | flops | bytes accessed | tf_op | source)
XLA Modules:
  0.0 403.7 jit_solution(9642668399519680433)
XLA Ops:
  7.2 0.8 broadcast_multiply_fusion
  8.1 0.8 copy.50
  9.4 0.8 copy.54
  10.4 18.0 %reduce-window.6 = s32[64,8,128]{2,1,0:T(8,128)S(1)} reduce-window(s32[64,8,128]{2,1,0:T(8,128)S(1)} %fusion.29, s32[]{:T(128)} %constant.18.clone.1), window={size=1x1x128 pad=0_0x0_0x127_0}, to_apply=%region_0.0 | reduce-window | flops 8323072 | bytes 524292 | tf_op jit(solution)/shard_map/reduce-window
  28.5 0.1 copy.52
  29.0 4.3 %scatter_custom_fusion.1 = s32[1280]{0:T(1024)S(1)} fusion(s32[1024]{0:T(1024)S(1)} %bitcast.61, s32[1024]{0:T(1024)S(1)} %iota.11, s32[]{:T(128)} %constant.18.clone.1), kind=kCustom, calls=%fused_computation.64 | custom fusion | bytes 5124 | tf_op jit(solution)/shard_map/scatter | solution.py:99
  33.4 4.3 %scatter_custom_fusion = s32[1280]{0:T(1024)S(1)} fusion(s32[1024]{0:T(1024)S(1)} %bitcast.62, s32[1024]{0:T(1024)S(1)} %broadcast.79, s32[]{:T(128)} %constant.18.clone.1), kind=kCustom, calls=%fused_computation.67 | custom fusion | bytes 5124 | tf_op jit(solution)/shard_map/scatter | solution.py:100
  37.8 6.1 %gather_fusion.1 = bf16[1280,2048]{1,0:T(8,128)(2,1)} fusion(bf16[256,2048]{1,0:T(8,128)(2,1)S(1)} %copy-done.1, s32[2048]{0:T(1024)S(1)} %get-tuple-element.42), kind=kCustom, calls=%fused_computation.1 | custom fusion | bytes 10490880 | tf_op jit(solution)/shard_map/gather | solution.py:105
  43.9 6.1 %gather_fusion = bf16[1280,2048]{1,0:T(8,128)(2,1)} fusion(bf16[256,2048]{1,0:T(8,128)(2,1)S(1)} %copy-done.2, s32[2048]{0:T(1024)S(1)} %get-tuple-element.42), kind=kCustom, calls=%fused_computation | custom fusion | bytes 10490880 | tf_op jit(solution)/shard_map/gather | solution.py:104
  50.0 5.0 %gather_fusion.2 = f32[1280]{0:T(1024)S(1)} fusion(f32[1024]{0:T(1024)S(1)} %reshape.79, s32[2048]{0:T(1024)S(1)} %get-tuple-element.41), kind=kCustom, calls=%fused_computation.2 | custom fusion | bytes 15360 | tf_op jit(solution)/shard_map/gather | solution.py:106
  55.0 2.2 dynamic-slice_select_fusion.1
  57.2 1.9 pad_maximum_fusion
  59.2 5.2 %all_to_all.32 = bf16[64,20,1024]{2,1,0:T(8,128)(2,1)} reshape(bf16[1280,1024]{1,0:T(8,128)(2,1)} %pad_maximum_fusion) | data formatting | bytes 5242880 | tf_op jit(solution)/shard_map/all_to_all | solution.py:17
  64.4 86.2 %all_to_all.49 = bf16[64,20,1024]{2,1,0:T(8,128)(2,1)} all-to-all(bf16[64,20,1024]{2,1,0:T(8,128)(2,1)} %all_to_all.32), channel_id=1, replica_groups=mesh['ep_0'=8,'ep_1'=4,'ep_2'=2,'tp'=4] {'ep_0','ep_1','ep_2'}, dimensions={0} | all-to-all | bytes 5242880 | tf_op jit(solution)/shard_map/all_to_all | solution.py:17
  150.6 5.2 %all_to_all.34 = bf16[1280,1024]{1,0:T(8,128)(2,1)} reshape(bf16[64,20,1024]{2,1,0:T(8,128)(2,1)} %all_to_all.49) | data formatting | bytes 5242880 | tf_op jit(solution)/shard_map/all_to_all | solution.py:17
  155.8 1.9 fusion.36
  157.7 1.7 pad_maximum_fusion.1
  159.5 15.6 %all_to_all.50 = f32[64,20,1]{1,2,0:T(1,128)S(1)} all-to-all(f32[64,20,1]{1,2,0:T(1,128)S(1)} %bitcast.56), channel_id=1, replica_groups=mesh['ep_0'=8,'ep_1'=4,'ep_2'=2,'tp'=4] {'ep_0','ep_1','ep_2'}, dimensions={0} | all-to-all | bytes 10240 | tf_op jit(solution)/shard_map/all_to_all | solution.py:112
  175.1 0.5 broadcast.139
  175.6 0.7 reduce.5
  176.4 83.3 %all-gather.2.cloned.1.call-done = bf16[2560,2048]{1,0:T(8,128)(2,1)} async-done(((bf16[2560,512]{1,0:T(8,128)(2,1)}), bf16[2560,2048]{1,0:T(8,128)(2,1)}) %all-gather.2.cloned.1.call-update) | async-done | bytes 10485776 | tf_op jit(solution)/shard_map/all_gather | solution.py:23
  259.7 4.2 %fusion.6 = f32[1280,256]{1,0:T(8,128)S(1)} fusion(bf16[2560,2048]{1,0:T(8,128)(2,1)} %all-gather.2.cloned.1.call-done, bf16[1,2048,256]{2,1,0:T(8,128)(2,1)S(1)} %copy-done.3), kind=kOutput, calls=%fused_computation.17 | convolution fusion | flops 1342177280 | bytes 7602176 | tf_op jit(solution)/shard_map/dot_general | solution.py:123
  263.9 1.3 copy-done.4
  265.3 1.6 fusion.8
  266.8 3.5 select_convert_fusion
  270.3 1.6 fusion.23
  271.9 3.9 add_convert_fusion
  275.8 1.1 copy-done.6
  276.9 4.5 %fusion.1 = f32[1280]{0:T(1024)S(1)} fusion(bf16[2560,2048]{1,0:T(8,128)(2,1)} %all-gather.2.cloned.1.call-done, bf16[1280,256]{1,0:T(8,128)(2,1)S(1)} %copy-done.6, bf16[1,256,2048]{2,1,0:T(8,128)(2,1)} %param.13), kind=kOutput, calls=%fused_computation.10 | convolution fusion | flops 1355283200 | bytes 6951936 | tf_op jit(solution)/shard_map/dot_general | solution.py:138
  281.4 7.7 %all_to_all.51 = f32[4,1,1280]{2,1,0:T(1,128)S(1)} all-to-all(f32[4,1,1280]{2,1,0:T(1,128)S(1)} %broadcast_in_dim.51), channel_id=1, replica_groups=mesh['ep_0'=8,'ep_1'=4,'ep_2'=2,'tp'=4] {'tp'}, dimensions={0} | all-to-all | bytes 40960 | tf_op jit(solution)/shard_map/all_to_all | solution.py:32
  289.5 5.7 %all_to_all.52 = f32[2,1,640]{2,1,0:T(1,128)S(1)} all-to-all(f32[2,1,640]{2,1,0:T(1,128)S(1)} %reshape.154), channel_id=1, replica_groups=mesh['ep_0'=8,'ep_1'=4,'ep_2'=2,'tp'=4] {'ep_2'}, dimensions={0} | all-to-all | bytes 10240 | tf_op jit(solution)/shard_map/all_to_all | solution.py:55
  295.2 0.5 broadcast.141
  295.7 0.7 reduce.6
  296.4 0.7 copy.58
  297.2 9.5 %all-to-all-start.5 = ((f32[32,2,20]{2,1,0:T(2,128)}), f32[32,2,20]{2,1,0:T(2,128)S(1)}, u32[]{:S(2)}, u32[]{:S(2)}) async-start(f32[32,2,20]{2,1,0:T(2,128)} %copy.58), calls=%async_computation.6 | async-start | bytes 65536 | tf_op jit(solution)/shard_map/all_to_all | solution.py:55
  306.7 28.6 %reduce-scatter.2.cloned.1.call-done = bf16[1280,512]{1,0:T(8,128)(2,1)} async-done(((bf16[1280,2048]{1,0:T(8,128)(2,1)}), bf16[1280,512]{1,0:T(8,128)(2,1)}) %reduce-scatter.2.cloned.1.call-update) | async-done | bytes 1310736 | tf_op jit(solution)/shard_map/reduce_scatter | solution.py:143
  335.3 3.2 all_to_all.37
  338.4 10.8 %all-to-all-start.2 = ((bf16[64,20,512]{2,1,0:T(8,128)(2,1)}), bf16[64,20,512]{2,1,0:T(8,128)(2,1)}, u32[]{:S(2)}, u32[]{:S(2)}) async-start(bf16[64,20,512]{2,1,0:T(8,128)(2,1)} %all_to_all.37), calls=%async_computation.3 | async-start | bytes 3145728 | tf_op jit(solution)/shard_map/all_to_all | solution.py:145
  349.2 5.6 %convolution_bitcast_fusion = f32[1,256,2048]{2,1,0:T(8,128)} fusion(bf16[1280,256]{1,0:T(8,128)(2,1)S(1)} %copy-done.6, f32[1280]{0:T(1024)S(1)} %mul.64, bf16[2560,2048]{1,0:T(8,128)(2,1)} %all-gather.2.cloned.1.call-done), kind=kOutput, calls=%fused_computation.23 | convolution fusion | flops 1350041600 | bytes 8000512 | tf_op jit(solution)/shard_map/rf,rd->fd/dot_general | solution.py:132
  354.9 5.5 %fusion.13 = f32[1,2048,256]{2,1,0:T(8,128)} fusion(bf16[1280,256]{1,0:T(8,128)(2,1)S(1)} %get-tuple-element.32, bf16[2560,2048]{1,0:T(8,128)(2,1)} %all-gather.2.cloned.1.call-done), kind=kOutput, calls=%fused_computation.22 | convolution fusion | flops 1342177280 | bytes 7995392 | tf_op jit(solution)/shard_map/rd,rf->df/dot_general | solution.py:130
  360.4 3.0 fusion.10
  363.5 6.2 %gather_fusion.4 = f32[1024]{0:T(1024)S(1)} fusion(f32[1280]{0:T(1024)S(1)} %reshape_reshape.7, s32[1024]{0:T(1024)S(1)} %broadcast_clamp_fusion), kind=kCustom, calls=%fused_computation.4 | custom fusion | bytes 12288 | tf_op jit(solution)/shard_map/gather | solution.py:151
  369.8 0.7 copy.59
  370.5 17.7 %all-to-all-done.2 = bf16[64,20,512]{2,1,0:T(8,128)(2,1)} async-done(((bf16[64,20,512]{2,1,0:T(8,128)(2,1)}), bf16[64,20,512]{2,1,0:T(8,128)(2,1)}, u32[]{:S(2)}, u32[]{:S(2)}) %all-to-all-start.2) | async-done | bytes 1310752 | tf_op jit(solution)/shard_map/all_to_all | solution.py:145
  388.2 2.3 all_to_all.39
  390.5 4.0 gather_fusion.3
  394.4 0.3 reshape.80
  394.7 2.1 reduce_sum.43
  (53 shorter events, 2.1 us)
Async XLA Ops:
  7.2 256.8 %copy-start = (bf16[1,2048,256]{2,1,0:T(8,128)(2,1)S(1)}, bf16[1,2048,256]{2,1,0:T(8,128)(2,1)}, u32[]{:S(2)}) copy-start(bf16[1,2048,256]{2,1,0:T(8,128)(2,1)} %param.11) | copy-start | bytes 3145732
  7.2 30.6 %copy-start.1 = (bf16[256,2048]{1,0:T(8,128)(2,1)S(1)}, bf16[256,2048]{1,0:T(8,128)(2,1)}, u32[]{:S(2)}) copy-start(bf16[256,2048]{1,0:T(8,128)(2,1)} %param.10) | copy-start | bytes 3145732
  7.2 252.5 %all-gather.2.cloned.1.call-start = ((), (), s32[]{:S(2)}) async-start(), calls=%async_computation.7 | async-start | bytes 13107200 | tf_op jit(solution)/shard_map/all_gather | solution.py:23
  37.7 6.1 %copy-start.2 = (bf16[256,2048]{1,0:T(8,128)(2,1)S(1)}, bf16[256,2048]{1,0:T(8,128)(2,1)}, u32[]{:S(2)}) copy-start(bf16[256,2048]{1,0:T(8,128)(2,1)} %param.7) | copy-start | bytes 3145732
  159.3 100.4 %copy-start.3 = (bf16[1,2048,256]{2,1,0:T(8,128)(2,1)S(1)}, bf16[1,2048,256]{2,1,0:T(8,128)(2,1)}, u32[]{:S(2)}) copy-start(bf16[1,2048,256]{2,1,0:T(8,128)(2,1)} %param.12) | copy-start | bytes 3145732
  159.4 175.9 %reduce-scatter.2.cloned.1.call-start = ((), (), s32[]{:S(2)}) async-start(), calls=%async_computation.8 | async-start | bytes 6553600 | tf_op jit(solution)/shard_map/reduce_scatter | solution.py:143
  259.7 5.5 %copy-start.4 = (bf16[2560,2048]{1,0:T(8,128)(2,1)S(1)}, bf16[2560,2048]{1,0:T(8,128)(2,1)}, u32[]{:S(2)}) copy-start(bf16[2560,2048]{1,0:T(8,128)(2,1)} %all-gather.2.cloned.1.call-done) | copy-start | bytes 31457284
  265.3 1.6 copy-start.5
  275.8 1.1 copy-start.6
  297.2 41.3 %all-to-all-start.5 = ((f32[32,2,20]{2,1,0:T(2,128)}), f32[32,2,20]{2,1,0:T(2,128)S(1)}, u32[]{:S(2)}, u32[]{:S(2)}) async-start(f32[32,2,20]{2,1,0:T(2,128)} %copy.58), calls=%async_computation.6 | async-start | bytes 65536 | tf_op jit(solution)/shard_map/all_to_all | solution.py:55
  338.4 49.7 %all-to-all-start.2 = ((bf16[64,20,512]{2,1,0:T(8,128)(2,1)}), bf16[64,20,512]{2,1,0:T(8,128)(2,1)}, u32[]{:S(2)}, u32[]{:S(2)}) async-start(bf16[64,20,512]{2,1,0:T(8,128)(2,1)} %all_to_all.37), calls=%async_computation.3 | async-start | bytes 3145728 | tf_op jit(solution)/shard_map/all_to_all | solution.py:145
  349.2 11.2 %slice-start = ((s8[10485760]{0:T(1024)(128)(4,1)}), s8[4194304]{0:T(1024)(128)(4,1)S(1)}, s32[]{:S(2)}) async-start(s8[10485760]{0:T(1024)(128)(4,1)} %bitcast.64), calls=%async_computation.9 | async-start | bytes 8388608
  349.2 11.2 %slice-start.1 = ((s8[10485760]{0:T(1024)(128)(4,1)}), s8[4194304]{0:T(1024)(128)(4,1)S(1)}, s32[]{:S(2)}) async-start(s8[10485760]{0:T(1024)(128)(4,1)} %bitcast.64), calls=%async_computation.10 | async-start | bytes 8388608
  354.9 5.5 %slice-start.2 = ((s8[10485760]{0:T(1024)(128)(4,1)}), s8[2097152]{0:T(1024)(128)(4,1)S(1)}, s32[]{:S(2)}) async-start(s8[10485760]{0:T(1024)(128)(4,1)} %bitcast.64), calls=%async_computation.11 | async-start | bytes 4194304
Sparse Core Ops, SparseCore 0:
  159.5 100.2 all-gather.1
  276.0 59.2 reduce-scatter.1
where the time goes:
time: 405 us; the launch traced here: 404 us
  waiting for transfers between devices  130 us (32%)
  blocking collectives  115 us (28%)
  local copies, waits for them, and re-layouts  62.2 us (15%)
  matrix products  33.4 us (8%)
  other arithmetic  28.5 us (7%)
  starting transfers between devices  20.4 us (5%)
  between operations  14.4 us (4%)
    all_to_all x1, blocking collectives, in_one_piece(): lax.all_to_all(both, axis, split_axis=split_dim, concat_axis=concat_dim,...  86.2 us
    all_gather x1, waiting for transfers between devices, in_one_piece_2(): result, at, outs = (lax.all_gather(both, axis, axis=dim, tiled=True), 0, [])  83.3 us
    reduce_scatter x1, waiting for transfers between devices, local(): lax.psum_scatter(all_rows, 'tp', scatter_dimension=1, tiled=True)  28.6 us
    another operation x3, other arithmetic  18.2 us
    all_to_all x1, waiting for transfers between devices, local(): lax.all_to_all(row_sum.astype(jnp.bfloat16), EP, split_axis=0, concat_axi...  17.7 us
    all_to_all x1, blocking collectives, local(): lax.all_to_all(send_weights, EP, split_axis=0, concat_axis=0, tiled=True)  15.6 us
    all_to_all x1, starting transfers between devices, local(): lax.all_to_all(row_sum.astype(jnp.bfloat16), EP, split_axis=0, concat_axi...  10.8 us
    all_to_all x2, local copies, waits for them, and re-layouts, in_one_piece(): lax.all_to_all(both, axis, split_axis=split_dim, concat_axis=concat_dim,...  10.4 us
  transfers between devices with their start and end apart: 4, of which 3 were waited for; matrix products, arithmetic and copies ran while one was open for 7% of the time, Pallas kernels for 0%

commit v1 on v0

v1 whole, which is shorter than its diff:
```python
import functools

import jax
import jax.numpy as jnp
from jax import lax
from jax.experimental import pallas as pl
from jax.experimental.pallas import tpu as pltpu
from jax.sharding import PartitionSpec as P

MESH = pl.DeviceIdType.MESH
BF16, F32 = jnp.bfloat16, jnp.float32
HIGH = lax.Precision.HIGHEST

CORES = 2
CHIPS_X = 4
MAIN = 16
REST = 4
SLOPE = 1.702
LIMIT = 7.0
AHEAD = 3


def nt(a, b, precision=None):
    return lax.dot_general(a, b, (((1,), (1,)), ((), ())), precision=precision, preferred_element_type=F32)


def tn(a, b, precision=None):
    return lax.dot_general(a, b, (((0,), (0,)), ((), ())), precision=precision, preferred_element_type=F32)


def nn(a, b, precision=None):
    return lax.dot_general(a, b, (((1,), (0,)), ((), ())), precision=precision, preferred_element_type=F32)


def iota(shape, dim):
    return lax.broadcasted_iota(jnp.int32, shape, dim)


def ranks(routes, lanes):
    tokens = routes.shape[0]
    expert = iota((tokens, lanes), 1)
    named = jnp.zeros((tokens, lanes), F32)
    for k in range(routes.shape[1]):
        named = named + jnp.where(routes[:, k : k + 1] == expert, 1.0, 0.0)
    earlier = jnp.where(iota((tokens, tokens), 0) >= iota((tokens, tokens), 1), 1.0, 0.0).astype(BF16)
    upto = nn(earlier, named.astype(BF16))
    return upto * named


def dispatch_kernel(experts, tp_ref, routes_ref, weights_ref, tokens_ref, grads_ref, s_ref):
    routes = routes_ref[...]
    weights = weights_ref[...]
    count = routes.shape[0]
    lanes = max(128, experts)
    expert = iota((count, lanes), 1)
    rank = ranks(routes, lanes)
    weight = jnp.zeros((count, lanes), F32)
    for k in range(routes.shape[1]):
        weight = weight + jnp.where(routes[:, k : k + 1] == expert, weights[:, k : k + 1], 0.0)
    rank_t = rank.T
    weight_t = weight.T
    x = tokens_ref[...]
    dy = grads_ref[...]
    width = x.shape[1]
    piece = width // 2
    some = min(16, experts)
    rows = some * MAIN
    for first in range(0, experts, some):
        rk = jnp.broadcast_to(rank_t[first : first + some][:, None, :], (some, MAIN, count)).reshape(rows, count)
        wt = jnp.broadcast_to(weight_t[first : first + some][:, None, :], (some, MAIN, count)).reshape(rows, count)
        row = (iota((rows, count), 0) & (MAIN - 1)).astype(F32)
        pick = rk == row + 1.0
        hot = jnp.where(pick, 1.0, 0.0).astype(BF16)
        scale = jnp.sum(jnp.where(pick, wt, 0.0), axis=1, keepdims=True)
        at = pl.ds(first * MAIN, rows)
        s_ref[at, 0:width] = nn(hot, x).astype(BF16)
        s_ref[at, width : 2 * width] = (nn(hot, dy) * scale).astype(BF16)
        sub = (iota((rows, count), 0) & (REST - 1)).astype(F32)
        pick = rk == sub + (1.0 + MAIN)
        hot = jnp.where(pick, 1.0, 0.0).astype(BF16)
        scale = jnp.sum(jnp.where(pick, wt, 0.0), axis=1, keepdims=True)
        which = (iota((rows, piece), 0) & (MAIN - 1)) // REST
        out = jnp.where(
            which < 2,
            jnp.where(which == 0, nn(hot, x[:, :piece]), nn(hot, x[:, piece:])),
            jnp.where(which == 2, nn(hot, dy[:, :piece]), nn(hot, dy[:, piece:])) * scale,
        )
        s_ref[at, 2 * width : 2 * width + piece] = out.astype(BF16)


def combine_kernel(experts, routes_ref, weights_ref, bk_ref, q_ref, grad_ref, gate_ref):
    routes = routes_ref[...]
    weights = weights_ref[...]
    count = routes.shape[0]
    lanes = max(128, experts)
    rank = ranks(routes, lanes)
    slots = experts * MAIN
    spread = jnp.where(iota((lanes, slots), 1) // MAIN == iota((lanes, slots), 0), 1.0, 0.0).astype(BF16)
    rk = nn(rank.astype(BF16), spread)
    lane = iota((count, slots), 1) & (MAIN - 1)
    width = bk_ref.shape[1] * 4 // 5
    piece = width // REST
    hot = jnp.where(rk == lane.astype(F32) + 1.0, 1.0, 0.0).astype(BF16)
    total = nn(hot, bk_ref[:, 0:width])
    late = rk == (lane & (REST - 1)).astype(F32) + (1.0 + MAIN)
    for q in range(REST):
        hot = jnp.where(late & (lane // REST == q), 1.0, 0.0).astype(BF16)
        at = slice(q * piece, (q + 1) * piece)
        grad_ref[:, at] = (total[:, at] + nn(hot, bk_ref[:, width : width + piece])).astype(BF16)
    expert = iota((count, lanes), 1)
    products = q_ref[...]
    for k in range(routes.shape[1]):
        mine = routes[:, k : k + 1] == expert
        hot = jnp.where(mine, 1.0, 0.0)
        slot = jnp.sum(jnp.where(mine, rank, 0.0), axis=1, keepdims=True)
        found = nn(hot[:, :experts], products, HIGH)
        chosen = jnp.where(iota(found.shape, 1).astype(F32) + 1.0 == slot, found, 0.0)
        gate_ref[:, k : k + 1] = jnp.sum(chosen, axis=1, keepdims=True) / weights[:, k : k + 1]


def exchange_kernel(
    nz, nj, ny,
    s, wg, wu, wd,
    bk_out, q_out, dwg, dwu, dwd,
    m, xa, da, ga, ua, ha, rt, ra, rb, rc, bo, pq, bk, qin, qy,
    ep_send, ep_recv, y_send, y_recv, f_send, f_recv, ra_send, ra_recv, rb_send, rb_recv, back_send, back_recv,
    q_send, q_recv, qy_send, qy_recv,
):
    nx = nj // CORES
    me = lax.axis_index("ep")
    y = lax.axis_index("tp")
    z, j = lax.div(me, nj), lax.rem(me, nj)
    x, core = lax.div(j, CORES), lax.rem(j, CORES)
    right, left, far = lax.rem(y + 1, ny), lax.rem(y + ny - 1, ny), lax.rem(y + 2, ny)
    width = rt.shape[-1]
    piece = width // 2
    back_piece = width // REST
    main = nj * MAIN
    rest = nj * REST
    rows = main + rest
    half = rows // 2
    half_main = main // 2
    groups = nz

    def remote(src, dst, send, recv, ep, tp):
        return pltpu.make_async_remote_copy(
            src_ref=src, dst_ref=dst, send_sem=send, recv_sem=recv, device_id=(ep, tp), device_id_type=MESH
        )

    def await_bytes(ref, sem):
        pltpu.make_async_copy(ref, ref, sem).wait()

    barrier = pltpu.get_barrier_semaphore()

    def greet(e, _):
        @pl.when(e != me)
        def _():
            pl.semaphore_signal(barrier, inc=1, device_id=(e, y), device_id_type=MESH)

        return 0

    lax.fori_loop(0, nz * nj, greet, 0)
    for other in (right, left, far):
        pl.semaphore_signal(barrier, inc=1, device_id=(me, other), device_id_type=MESH)
    pl.semaphore_wait(barrier, nz * nj - 1 + 3)

    def step_of(g):
        odd, half_g = lax.rem(g, 2), lax.div(g + 1, 2)
        return lax.rem(odd * half_g + (1 - odd) * (nz - half_g), nz)

    def other_j(o):
        return lax.rem(x + o // CORES, nx) * CORES + lax.rem(core + o % CORES, CORES)

    def tile(e):
        return pl.ds(pl.multiple_of(e * MAIN, MAIN), MAIN)

    def send_group(g, orders):
        zd = lax.rem(z + step_of(g), nz)
        for o in orders:
            dest = zd * nj + other_j(o)
            remote(s.at[tile(dest), :], m.at[g, y, tile(j), :], ep_send, ep_recv.at[g], dest, y).start()

    send_group(jnp.int32(0), range(1, nj))
    for g in range(1, min(AHEAD, groups)):
        send_group(jnp.int32(g), range(nj))
    m[0, y, tile(j), :] = s[tile(me), :]

    a, b = iota((main, main), 0), iota((main, main), 1)
    q_of, src_of, j_of = lax.div(a, rest), lax.div(lax.rem(a, rest), REST), lax.rem(a, REST)
    apart = jnp.where(b == src_of * MAIN + q_of * REST + j_of, 1.0, 0.0).astype(BF16)
    q_in, src_in, j_in = lax.div(b, rest), lax.div(lax.rem(b, rest), REST), lax.rem(b, REST)
    together = jnp.where(a == src_in * MAIN + q_in * REST + j_in, 1.0, 0.0).astype(BF16)
    r, lane = iota((rows, 128), 0), iota((rows, 128), 1)
    slot_of = jnp.where(r < main, lax.rem(r, MAIN), MAIN + lax.rem(r, REST))
    at_slot = lane == slot_of
    rr = iota((nj, rows), 1)
    from_src = jnp.where(rr < main, lax.div(rr, MAIN), lax.div(rr - main, REST)) == iota((nj, rows), 0)
    from_src = jnp.where(from_src, 1.0, 0.0)

    def arrive(g):
        @pl.when(g == 0)
        def _():
            await_bytes(m.at[0, y, pl.ds(0, main - MAIN), :], ep_recv.at[0])

        @pl.when(g > 0)
        def _():
            await_bytes(m.at[g, y], ep_recv.at[g])

        remote(m.at[g, y], m.at[g, y], y_send, y_recv.at[0, g], me, right).start()
        remote(m.at[g, y], m.at[g, y], y_send, y_recv.at[1, g], me, left).start()

    def forward(g):
        await_bytes(m.at[g, left], y_recv.at[0, g])
        low = m.at[g, left, pl.ds(0, half_main), :]
        remote(low, low, f_send, f_recv.at[0, g], me, right).start()
        await_bytes(m.at[g, right], y_recv.at[1, g])
        high = m.at[g, right, pl.ds(half_main, half_main), :]
        remote(high, high, f_send, f_recv.at[1, g], me, left).start()

    def compute(g):
        await_bytes(m.at[g, far, pl.ds(0, half_main), :], f_recv.at[0, g])
        await_bytes(m.at[g, far, pl.ds(half_main, half_main), :], f_recv.at[1, g])
        row0 = pl.multiple_of(g * rows, REST * nj)
        at_main, at_rest, at_all = pl.ds(row0, main), pl.ds(row0 + main, rest), pl.ds(row0, rows)
        for slab in range(ny):
            c0 = slab * width
            xa[at_main, c0 : c0 + width] = m[g, slab, :, 0:width]
            da[at_main, c0 : c0 + width] = m[g, slab, :, width : 2 * width]
            pieces = nn(apart, m[g, slab, :, 2 * width : 2 * width + piece]).astype(BF16)
            xa[at_rest, c0 : c0 + piece] = pieces[0:rest]
            xa[at_rest, c0 + piece : c0 + width] = pieces[rest : 2 * rest]
            da[at_rest, c0 : c0 + piece] = pieces[2 * rest : 3 * rest]
            da[at_rest, c0 + piece : c0 + width] = pieces[3 * rest : 4 * rest]
        gate_pre = nn(xa[at_all, :], wg[...])
        up_pre = nn(xa[at_all, :], wu[...])
        hidden_grad = nt(da[at_all, :], wd[...])
        glu = jnp.minimum(gate_pre, LIMIT)
        linear = jnp.clip(up_pre, -LIMIT, LIMIT)
        sigma = jax.nn.sigmoid(SLOPE * glu)
        active = glu * sigma
        hidden = (active * (linear + 1.0)).astype(BF16)
        slope = sigma + SLOPE * active * (1.0 - sigma)
        gpg = jnp.where(gate_pre < LIMIT, hidden_grad * (linear + 1.0) * slope, 0.0).astype(BF16)
        upg = jnp.where(jnp.abs(up_pre) < LIMIT, hidden_grad * active, 0.0).astype(BF16)
        ga[at_all, :] = gpg
        ua[at_all, :] = upg
        ha[at_all, :] = hidden
        for slab in range(ny):
            c0 = slab * width
            term = nt(gpg, wg[c0 : c0 + width, :]) + nt(upg, wu[c0 : c0 + width, :])
            rt[g, slab] = term.astype(BF16)
        low, high = pl.ds(0, half), pl.ds(half, half)
        remote(rt.at[g, far, low], ra.at[g, 0], ra_send, ra_recv.at[0, g], me, right).start()
        remote(rt.at[g, far, high], ra.at[g, 1], ra_send, ra_recv.at[1, g], me, left).start()
        remote(rt.at[g, right, high], rb.at[g, 0, high], rb_send, rb_recv.at[0, g], me, right).start()
        remote(rt.at[g, left, low], rb.at[g, 1, low], rb_send, rb_recv.at[1, g], me, left).start()
        product = jnp.sum(hidden.astype(F32) * hidden_grad, axis=1, keepdims=True)
        laid = nn(from_src, jnp.where(at_slot, product, 0.0), HIGH)
        for src in range(nj):
            pq[g, src] = laid[src : src + 1, :]
        zs = lax.rem(z - step_of(g) + nz, nz)
        for o in range(nj):
            to = other_j(o)

            def send_products(to=to):
                remote(pq.at[g, to], qin.at[me], q_send, q_recv, zs * nj + to, y).start()

            if o == 0:
                pl.when(g > 0)(send_products)
            else:
                send_products()

    def partly(g):
        low, high = pl.ds(0, half), pl.ds(half, half)
        await_bytes(ra.at[g, 0], ra_recv.at[0, g])
        rc[g, 0] = (ra[g, 0].astype(F32) + rt[g, right, low].astype(F32)).astype(BF16)
        remote(rc.at[g, 0], rb.at[g, 0, low], rb_send, rb_recv.at[0, g], me, right).start()
        await_bytes(ra.at[g, 1], ra_recv.at[1, g])
        rc[g, 1] = (ra[g, 1].astype(F32) + rt[g, left, high].astype(F32)).astype(BF16)
        remote(rc.at[g, 1], rb.at[g, 1, high], rb_send, rb_recv.at[1, g], me, left).start()

    def give_back(g):
        await_bytes(rb.at[g, 0], rb_recv.at[0, g])
        await_bytes(rb.at[g, 1], rb_recv.at[1, g])
        total = rt[g, y].astype(F32) + rb[g, 0].astype(F32) + rb[g, 1].astype(F32)
        done = total.astype(BF16)
        bo[g, :, 0:width] = done[0:main]
        stacked = jnp.concatenate(
            [done[main:rows, q * back_piece : (q + 1) * back_piece] for q in range(REST)], axis=0
        )
        bo[g, :, width : width + back_piece] = nn(together, stacked).astype(BF16)
        zs = lax.rem(z - step_of(g) + nz, nz)
        for o in range(nj):
            to = other_j(o)

            def send_rows(to=to):
                remote(bo.at[g, tile(to), :], bk.at[tile(me), :], back_send, back_recv, zs * nj + to, y).start()

            if o == 0:
                pl.when(g > 0)(send_rows)
            else:
                send_rows()

    def step(i, _):
        @pl.when(i + AHEAD < groups)
        def _():
            send_group(i + AHEAD, range(nj))

        pl.when(i < groups)(lambda: arrive(i))
        pl.when((i >= 1) & (i < groups + 1))(lambda: forward(i - 1))
        pl.when((i >= 2) & (i < groups + 2))(lambda: compute(i - 2))
        pl.when((i >= 3) & (i < groups + 3))(lambda: partly(i - 3))
        pl.when(i >= 4)(lambda: give_back(i - 4))
        return 0

    lax.fori_loop(0, groups + 4, step, 0)

    bk[tile(me), :] = bo[0, tile(j), :]
    qin[me] = pq[0, j]
    await_bytes(qin.at[pl.ds(0, nz * nj - 1)], q_recv)
    remote(qin, qy.at[0], qy_send.at[0], qy_recv.at[0], me, right).start()
    remote(qin, qy.at[1], qy_send.at[1], qy_recv.at[1], me, left).start()
    remote(qin, qy.at[2], qy_send.at[2], qy_recv.at[2], me, far).start()

    block = min(256, xa.shape[1])

    def weight_grads(i, _):
        at = pl.ds(pl.multiple_of(i * block, block), block)
        dwg[at, :] = tn(xa[:, at], ga[...])
        dwu[at, :] = tn(xa[:, at], ua[...])
        dwd[:, at] = tn(ha[...], da[:, at])
        return 0

    lax.fori_loop(0, xa.shape[1] // block, weight_grads, 0)

    await_bytes(bk.at[pl.ds(0, (nz * nj - 1) * MAIN), :], back_recv)
    bk_out[...] = bk[...]
    for k in range(3):
        await_bytes(qy.at[k], qy_recv.at[k])
        await_bytes(qin, qy_send.at[k])
    q_out[...] = qin[...] + qy[0] + qy[1] + qy[2]

    everything = pl.ds(0, (nz * nj - 1) * MAIN)
    await_bytes(s.at[everything, :], ep_send)
    for _ in range(2):
        await_bytes(m.at[:, 0], y_send)
        await_bytes(m.at[:, 0, pl.ds(0, half_main), :], f_send)
        await_bytes(ra.at[:, 0], ra_send)
        await_bytes(rb.at[:, 0], rb_send)
    await_bytes(bk.at[everything, :], back_send)
    await_bytes(qin.at[pl.ds(0, nz * nj - 1)], q_send)


def local(nz, nj, ny, tokens, routes, gate_weights, out_grad, w_gate, w_up, w_down):
    count, model = tokens.shape
    units = w_gate.shape[2]
    top = routes.shape[1]
    experts = nz * nj
    width = model // ny
    wide, back_wide = width * 5 // 2, width * 5 // 4
    vmem = pl.BlockSpec(memory_space=pltpu.VMEM)
    tp = lax.axis_index("tp").reshape(1)
    sent = pl.pallas_call(
        functools.partial(dispatch_kernel, experts),
        out_shape=jax.ShapeDtypeStruct((experts * MAIN, wide), BF16),
        grid_spec=pltpu.PrefetchScalarGridSpec(
            num_scalar_prefetch=1,
            grid=(1,),
            in_specs=[
                pl.BlockSpec((count, top), lambda i, t: (0, 0)),
                pl.BlockSpec((count, top), lambda i, t: (0, 0)),
                pl.BlockSpec((count, width), lambda i, t: (0, t[0])),
                pl.BlockSpec((count, width), lambda i, t: (0, t[0])),
            ],
            out_specs=pl.BlockSpec((experts * MAIN, wide), lambda i, t: (0, 0)),
        ),
        compiler_params=pltpu.CompilerParams(vmem_limit_bytes=40 << 20),
        name="dispatch",
    )(tp, routes, gate_weights, tokens, out_grad)

    groups, main, rows = nz, nj * MAIN, nj * (MAIN + REST)
    all_rows = groups * rows
    dma = pltpu.SemaphoreType.DMA
    back, products, dwg, dwu, dwd = pl.pallas_call(
        functools.partial(exchange_kernel, nz, nj, ny),
        out_shape=(
            jax.ShapeDtypeStruct((experts * MAIN, back_wide), BF16),
            jax.ShapeDtypeStruct((experts, 1, 128), F32),
            jax.ShapeDtypeStruct((model, units), F32),
            jax.ShapeDtypeStruct((model, units), F32),
            jax.ShapeDtypeStruct((units, model), F32),
        ),
        in_specs=[vmem] * 4,
        out_specs=(vmem,) * 5,
        scratch_shapes=[
            pltpu.VMEM((groups, ny, main, wide), BF16),
            pltpu.VMEM((all_rows, model), BF16),
            pltpu.VMEM((all_rows, model), BF16),
            pltpu.VMEM((all_rows, units), BF16),
            pltpu.VMEM((all_rows, units), BF16),
            pltpu.VMEM((all_rows, units), BF16),
            pltpu.VMEM((groups, ny, rows, width), BF16),
            pltpu.VMEM((groups, 2, rows // 2, width), BF16),
            pltpu.VMEM((groups, 2, rows, width), BF16),
            pltpu.VMEM((groups, 2, rows // 2, width), BF16),
            pltpu.VMEM((groups, main, back_wide), BF16),
            pltpu.VMEM((groups, nj, 1, 128), F32),
            pltpu.VMEM((experts * MAIN, back_wide), BF16),
            pltpu.VMEM((experts, 1, 128), F32),
            pltpu.VMEM((3, experts, 1, 128), F32),
            dma, dma((groups,)),
            dma, dma((2, groups)),
            dma, dma((2, groups)),
            dma, dma((2, groups)),
            dma, dma((2, groups)),
            dma, dma,
            dma, dma,
            dma((3,)), dma((3,)),
        ],
        compiler_params=pltpu.CompilerParams(
            collective_id=0, has_side_effects=True, vmem_limit_bytes=63 << 20
        ),
        name="exchange",
    )(sent, w_gate[0], w_up[0], w_down[0])

    token_grad, gate_grad = pl.pallas_call(
        functools.partial(combine_kernel, experts),
        out_shape=(
            jax.ShapeDtypeStruct((count, width), BF16),
            jax.ShapeDtypeStruct((count, top), F32),
        ),
        in_specs=[vmem] * 4,
        out_specs=(vmem, vmem),
        compiler_params=pltpu.CompilerParams(vmem_limit_bytes=40 << 20),
        name="combine",
    )(routes, gate_weights, back, products.reshape(experts, 128))
    return token_grad, gate_grad, dwg[None], dwu[None], dwd[None]


def solution(mesh):
    nj = CHIPS_X * CORES
    nz, ny = mesh.shape["ep"] // nj, mesh.shape["tp"]
    in_specs = (
        P("ep", None),
        P("ep", None),
        P("ep", None),
        P("ep", None),
        P("ep", None, "tp"),
        P("ep", None, "tp"),
        P("ep", "tp", None),
    )
    out_specs = (P("ep", "tp"), P("ep", None), P("ep", None, "tp"), P("ep", None, "tp"), P("ep", "tp", None))
    return jax.shard_map(
        functools.partial(local, nz, nj, ny), mesh=mesh, in_specs=in_specs, out_specs=out_specs, check_vma=False
    )
```

time: 405 us -> 199 us (0.49)
  Pallas kernels: 0 us -> 183 us
  waiting for transfers between devices: 130 us -> 0 us
  blocking collectives: 115 us -> 0 us
  local copies, waits for them, and re-layouts: 62.2 us -> 15.2 us
  matrix products: 33.4 us -> 0 us
  other arithmetic: 28.5 us -> 0 us
  starting transfers between devices: 20.4 us -> 0 us
  between operations: 14.4 us -> 0.7 us
    pallas_call x0 -> x3, Pallas kernels: none -> 183 us  [the longest x1 179 us: local(): pl.pallas_call(functools.partial(exchange_kernel, nz, nj, ny), out_shape=...]
    all_to_all x4 -> x0, blocking collectives: 115 us -> none  [the longest x1 86.2 us: in_one_piece(): lax.all_to_all(both, axis, split_axis=split_dim, concat_axis=concat_dim,...]
    all_gather x1 -> x0, waiting for transfers between devices: 83.3 us -> none  [in_one_piece_2(): result, at, outs = (lax.all_gather(both, axis, axis=dim, tiled=True), 0, [])]
    dot_general x9 -> x0, matrix products: 33.4 us -> none  [the longest x1 5.62 us: local(): jnp.einsum('rf,rd->fd', hidden, scaled, preferred_element_type=jnp.float32)]
    reduce_scatter x1 -> x0, waiting for transfers between devices: 28.6 us -> none  [local(): lax.psum_scatter(all_rows, 'tp', scatter_dimension=1, tiled=True)]
    gather x5 -> x0, local copies, waits for them, and re-layouts: 27.3 us -> none  [the longest x1 6.15 us: local(): gate_grad = back_products[target].reshape(token_count, top_count)]
    all_to_all x2 -> x0, starting transfers between devices: 20.3 us -> none  [the longest x1 10.8 us: local(): lax.all_to_all(row_sum.astype(jnp.bfloat16), EP, split_axis=0, concat_axi...]
    another operation x3 -> x0, other arithmetic: 18.2 us -> none
  transfers between devices with their start and end apart: 4 -> 0, of which waited for: 3 -> 0; matrix products, arithmetic and copies ran while one was open for 7% -> 0% of each run, Pallas kernels for 0% -> 0%
where the time goes in v1:
time: 199 us
  Pallas kernels  183 us (92%)
  local copies, waits for them, and re-layouts  15.2 us (8%)
    pallas_call x1, Pallas kernels, local(): pl.pallas_call(functools.partial(exchange_kernel, nz, nj, ny), out_shape=...  179 us
    unnamed x20, local copies, waits for them, and re-layouts  15.2 us

profile of v1, /device:TPU:1, one launch (start us, length us, event | category | flops | bytes accessed | tf_op | source)
XLA Modules:
  0.0 198.6 jit_solution(3660682005960889521)
XLA Ops:
  0.6 0.8 copy.14.routes_ref
  1.5 0.8 copy.15.weights_ref
  2.3 0.0 copy-start.2
  2.3 1.2 copy-done.2
  3.5 0.0 copy-start.3
  3.5 1.2 copy-done.3
  4.7 1.9 dispatch.1.s
  6.6 0.0 copy-start
  6.6 1.5 copy-done
  8.2 178.5 %exchange.1 = (bf16[1024,640]{1,0:T(8,128)(2,1)}, f32[64,1,128]{2,1,0:T(1,128)}, f32[2048,256]{1,0:T(8,128)}, f32[2048,256]{1,0:T(8,128)}, f32[256,2048]{1,0:T(8,128)}) custom-call(bf16[1024,1280]{1,0:T(8,128)(2,1)} %copy-done, bf16[2048,256]{1,0:T(8,128)(2,1)} %bitcast.12, bf16[2048,256]{1,0:T(8,128)(2,1)} %bitcast.13, bf16[256,2048]{1,0:T(8,128)(2,1)} %bitcast.14), custom_call_target="tpu_custom_call" | custom-call | tf_op jit(solution)/shard_map/exchange/pallas_call | solution.py:384
  186.7 0.0 copy-start.1
  186.7 1.3 copy-done.1
  188.0 0.0 copy-start.4
  188.0 0.8 copy-done.4
  188.8 2.3 %combine.1 = (bf16[256,512]{1,0:T(8,128)(2,1)}, f32[256,4]{1,0:T(8,128)S(1)}) custom-call(s32[256,4]{1,0:T(8,128)S(1)} %copy.14.routes_ref, f32[256,4]{1,0:T(8,128)S(1)} %copy.15.weights_ref, bf16[1024,640]{1,0:T(8,128)(2,1)S(1)} %copy-done.1, f32[64,128]{1,0:T(8,128)S(1)} %bitcast.8), custom_call_target="tpu_custom_call" | custom-call | tf_op jit(solution)/shard_map/combine/pallas_call | solution.py:426
  191.0 0.7 copy.16
  191.7 0.0 copy-start.6
  191.7 3.2 %copy.20 = f32[1,2048,256]{2,1,0:T(8,128)} copy(f32[1,2048,256]{2,1,0:T(8,128)} %bitcast.11) | data formatting | bytes 4194304
  194.9 0.0 copy-done.6
  194.9 0.0 copy-start.5
  194.9 1.3 copy.21
  196.2 1.0 copy-done.5
  197.2 1.3 copy.22
Async XLA Ops:
  2.3 1.2 copy-start.2
  3.5 1.2 copy-start.3
  6.6 1.5 copy-start
  186.7 1.3 copy-start.1
  188.0 0.8 copy-start.4
  191.7 3.2 %copy-start.6 = (f32[2048,256]{1,0:T(8,128)S(1)}, f32[2048,256]{1,0:T(8,128)}, u32[]{:S(2)}) copy-start(f32[2048,256]{1,0:T(8,128)} %get-tuple-element.17) | copy-start | bytes 6291460
  194.9 2.3 %copy-start.5 = (f32[256,2048]{1,0:T(8,128)S(1)}, f32[256,2048]{1,0:T(8,128)}, u32[]{:S(2)}) copy-start(f32[256,2048]{1,0:T(8,128)} %get-tuple-element.18) | copy-start | bytes 6291460

commit v2 on v1

v2 whole, which is shorter than its diff:
```python
import functools

import jax
import jax.numpy as jnp
from jax import lax
from jax.experimental import pallas as pl
from jax.experimental.pallas import tpu as pltpu
from jax.sharding import PartitionSpec as P

MESH = pl.DeviceIdType.MESH
BF16, F32 = jnp.bfloat16, jnp.float32
HIGH = lax.Precision.HIGHEST

CORES = 2
CHIPS_X = 4
MAIN = 16
REST = 4
SLOPE = 1.702
LIMIT = 7.0
DISTANCE = (0, 2, -2, 1, -1, 3, -3, 4)
NEAR = (3, 4)


def nt(a, b, precision=None):
    return lax.dot_general(a, b, (((1,), (1,)), ((), ())), precision=precision, preferred_element_type=F32)


def tn(a, b, precision=None):
    return lax.dot_general(a, b, (((0,), (0,)), ((), ())), precision=precision, preferred_element_type=F32)


def nn(a, b, precision=None):
    return lax.dot_general(a, b, (((1,), (0,)), ((), ())), precision=precision, preferred_element_type=F32)


def iota(shape, dim):
    return lax.broadcasted_iota(jnp.int32, shape, dim)


def ranks(routes, experts):
    top, tokens = routes.shape
    expert = iota((experts, tokens), 0)
    named = jnp.zeros((experts, tokens), F32)
    for k in range(top):
        named = named + jnp.where(routes[k : k + 1, :] == expert, 1.0, 0.0)
    earlier = jnp.where(iota((tokens, tokens), 0) <= iota((tokens, tokens), 1), 1.0, 0.0).astype(BF16)
    return nn(named.astype(BF16), earlier) * named


def exchange_kernel(
    nz, nj, ny,
    routes, weights, tokens, grads, wg_hbm, wu_hbm, wd_hbm,
    bk, q_out, dwg_hbm, dwu_hbm, dwd_hbm,
    x_in, dy_in, wg, wu, wd, rank, weight, s, s_near, s_here, m, xa, da, ga, ua, ha, rt, ra, rb, rc, bo, pq, qin, qy,
    dwg, dwu, dwd,
    in_sem, w_sem, own_sem, dw_sem,
    ep_send, ep_recv, near_send, near_recv, y_send, y_recv, f_send, f_recv, ra_send, ra_recv, rb_send, rb_recv,
    back_send, back_recv, q_send, q_recv, qy_send, qy_recv,
):
    nx = nj // CORES
    experts = nz * nj
    me = lax.axis_index("ep")
    y = lax.axis_index("tp")
    z, j = lax.div(me, nj), lax.rem(me, nj)
    x, core = lax.div(j, CORES), lax.rem(j, CORES)
    right, left, far = lax.rem(y + 1, ny), lax.rem(y + ny - 1, ny), lax.rem(y + 2, ny)
    width = rt.shape[-1]
    piece = width // REST
    packed = width + piece
    main = nj * MAIN
    rest = nj * REST
    rows = main + rest
    half = rows // 2
    half_main = main // 2
    groups = nz
    count = x_in.shape[0]

    def remote(src, dst, send, recv, ep, tp):
        return pltpu.make_async_remote_copy(
            src_ref=src, dst_ref=dst, send_sem=send, recv_sem=recv, device_id=(ep, tp), device_id_type=MESH
        )

    def await_bytes(ref, sem):
        pltpu.make_async_copy(ref, ref, sem).wait()

    loads = [pltpu.make_async_copy(a, b, in_sem.at[k]) for k, (a, b) in enumerate(((tokens, x_in), (grads, dy_in)))]
    loads += [
        pltpu.make_async_copy(a, b, w_sem.at[k]) for k, (a, b) in enumerate(((wg_hbm, wg), (wu_hbm, wu), (wd_hbm, wd)))
    ]
    for load in loads:
        load.start()

    barrier = pltpu.get_barrier_semaphore()

    def greet(e, _):
        @pl.when(e != me)
        def _():
            pl.semaphore_signal(barrier, inc=1, device_id=(e, y), device_id_type=MESH)

        return 0

    lax.fori_loop(0, experts, greet, 0)
    for other in (right, left, far):
        pl.semaphore_signal(barrier, inc=1, device_id=(me, other), device_id_type=MESH)

    distances = sum((d % nz) << (4 * k) for k, d in enumerate(DISTANCE[:groups]))

    def step_of(g):
        if isinstance(g, int):
            return DISTANCE[g] % nz
        return lax.rem(lax.shift_right_logical(jnp.int32(distances), 4 * g), 16)

    def other_j(o):
        return lax.rem(x + o // CORES, nx) * CORES + lax.rem(core + o % CORES, CORES)

    def tile(e):
        return pl.ds(pl.multiple_of(e * MAIN, MAIN), MAIN)

    rank[...] = ranks(routes[...], experts)
    expert = iota((experts, count), 0)
    weight_of = jnp.zeros((experts, count), F32)
    for k in range(routes.shape[0]):
        weight_of = weight_of + jnp.where(routes[k : k + 1, :] == expert, weights[k : k + 1, :], 0.0)
    weight[...] = weight_of
    loads[0].wait()
    loads[1].wait()

    row = iota((main, count), 0)
    quarter = lax.div(lax.rem(iota((main, piece), 0), MAIN), REST)
    own_columns = pl.ds(pl.multiple_of(y * width, width), width)

    def pickers(g):
        zd = lax.rem(z + step_of(g), nz)
        at = pl.ds(pl.multiple_of(zd * nj, nj), nj)
        rk = jnp.broadcast_to(rank[at, :][:, None, :], (nj, MAIN, count)).reshape(main, count)
        wt = jnp.broadcast_to(weight[at, :][:, None, :], (nj, MAIN, count)).reshape(main, count)
        out = []
        for slot in (lax.rem(row, MAIN) + 1, lax.rem(row, REST) + 1 + MAIN):
            pick = rk == slot.astype(F32)
            hot = jnp.where(pick, 1.0, 0.0).astype(BF16)
            out.append((hot, jnp.sum(jnp.where(pick, wt, 0.0), axis=1, keepdims=True)))
        return out

    def pack(out, values, picks, scaled):
        (hot, scale), (hot_rest, scale_rest) = picks
        body = nn(hot, values)
        tail = nn(hot_rest, values)
        edge = tail[:, 0:piece]
        for q in range(1, REST):
            edge = jnp.where(quarter == q, tail[:, q * piece : (q + 1) * piece], edge)
        if scaled:
            body, edge = body * scale, edge * scale_rest
        out[:, 0:width] = body.astype(BF16)
        out[:, width:packed] = edge.astype(BF16)

    def pack_own(g, _):
        picks = pickers(g)
        pack(s.at[g, 0], x_in[:, own_columns], picks, False)
        pack(s.at[g, 1], dy_in[:, own_columns], picks, True)
        return 0

    def send_own(g):
        zd = lax.rem(z + step_of(g), nz)
        for o in range(nj):
            to = other_j(o)
            dest = zd * nj + to
            if g in NEAR:
                src, dst = s.at[g, 1, tile(to), :], m.at[g, y, 1, tile(j), :]
            else:
                src, dst = s.at[g, :, tile(to), :], m.at[g, y, :, tile(j), :]
            remote(src, dst, ep_send, ep_recv.at[g], dest, y).start()

    lax.fori_loop(1, groups, pack_own, 0)
    pl.semaphore_wait(barrier, experts - 1 + 3)
    for g in (3, 4, 1, 2):
        send_own(g)

    picks = pickers(0)
    for slab in range(ny):
        pack(s_here.at[slab, 0], x_in[:, slab * width : (slab + 1) * width], picks, False)
        pack(s_here.at[slab, 1], dy_in[:, slab * width : (slab + 1) * width], picks, True)
    for o in range(1, nj):
        to = other_j(o)
        remote(
            s_here.at[:, :, tile(to), :], m.at[0, :, :, tile(j), :], ep_send, ep_recv.at[0], z * nj + to, y
        ).start()
    for slab in range(ny):
        for k in range(2):
            m[0, slab, k, tile(j), :] = s_here[slab, k, tile(j), :]
    for g in (5, 6):
        send_own(g)
    for n, g in enumerate(NEAR):
        picks = pickers(g)
        for slab in range(ny):
            pack(s_near.at[n, slab], x_in[:, slab * width : (slab + 1) * width], picks, False)
        zd = lax.rem(z + step_of(g), nz)
        for o in range(nj):
            to = other_j(o)
            remote(
                s_near.at[n, :, tile(to), :], m.at[g, :, 0, tile(j), :], near_send, near_recv.at[n], zd * nj + to, y
            ).start()
    send_own(7)

    a, b = iota((main, main), 0), iota((main, main), 1)
    q_of, src_of, j_of = lax.div(a, rest), lax.div(lax.rem(a, rest), REST), lax.rem(a, REST)
    apart = jnp.where(b == src_of * MAIN + q_of * REST + j_of, 1.0, 0.0).astype(BF16)
    q_in, src_in, j_in = lax.div(b, rest), lax.div(lax.rem(b, rest), REST), lax.rem(b, REST)
    together = jnp.where(a == src_in * MAIN + q_in * REST + j_in, 1.0, 0.0).astype(BF16)
    r, lane = iota((rows, 128), 0), iota((rows, 128), 1)
    slot_of = jnp.where(r < main, lax.rem(r, MAIN), MAIN + lax.rem(r, REST))
    at_slot = lane == slot_of
    rr = iota((nj, rows), 1)
    from_src = jnp.where(rr < main, lax.div(rr, MAIN), lax.div(rr - main, REST)) == iota((nj, rows), 0)
    from_src = jnp.where(from_src, 1.0, 0.0)

    def part(g, slab):
        return m.at[g, slab, 1] if g in NEAR else m.at[g, slab]

    def halves(g, slab):
        if g in NEAR:
            return [m.at[g, slab, 1, pl.ds(h * half_main, half_main), :] for h in range(2)]
        return [m.at[g, slab, :, pl.ds(h * half_main, half_main), :] for h in range(2)]

    def arrive(g):
        await_bytes(part(g, y), ep_recv.at[g])
        remote(part(g, y), part(g, y), y_send, y_recv.at[0, g], me, right).start()
        remote(part(g, y), part(g, y), y_send, y_recv.at[1, g], me, left).start()

    def forward(g):
        await_bytes(part(g, left), y_recv.at[0, g])
        low = halves(g, left)[0]
        remote(low, low, f_send, f_recv.at[0, g], me, right).start()
        await_bytes(part(g, right), y_recv.at[1, g])
        high = halves(g, right)[1]
        remote(high, high, f_send, f_recv.at[1, g], me, left).start()

    def gathered(g):
        @pl.when(g == 0)
        def _():
            await_bytes(m.at[0, :, :, pl.ds(0, main - MAIN), :], ep_recv.at[0])
            for load in loads[2:]:
                load.wait()

        for n, near in enumerate(NEAR):

            @pl.when(g == near)
            def _(n=n, near=near):
                await_bytes(m.at[near, :, 0], near_recv.at[n])
                for h in range(2):
                    await_bytes(halves(near, far)[h], f_recv.at[h, near])

        @pl.when((g != 0) & (g != NEAR[0]) & (g != NEAR[1]))
        def _():
            for h in range(2):
                await_bytes(m.at[g, far, :, pl.ds(h * half_main, half_main), :], f_recv.at[h, g])

    def compute(g):
        gathered(g)
        row0 = pl.multiple_of(g * rows, REST * nj)
        at_main, at_rest, at_all = pl.ds(row0, main), pl.ds(row0 + main, rest), pl.ds(row0, rows)
        for slab in range(ny):
            c0 = slab * width
            for k, out in enumerate((xa, da)):
                out[at_main, c0 : c0 + width] = m[g, slab, k, :, 0:width]
                pieces = nn(apart, m[g, slab, k, :, width:packed]).astype(BF16)
                for q in range(REST):
                    out[at_rest, c0 + q * piece : c0 + (q + 1) * piece] = pieces[q * rest : (q + 1) * rest]
        gate_pre = nn(xa[at_all, :], wg[...])
        up_pre = nn(xa[at_all, :], wu[...])
        hidden_grad = nt(da[at_all, :], wd[...])
        glu = jnp.minimum(gate_pre, LIMIT)
        linear = jnp.clip(up_pre, -LIMIT, LIMIT)
        sigma = jax.nn.sigmoid(SLOPE * glu)
        active = glu * sigma
        hidden = (active * (linear + 1.0)).astype(BF16)
        slope = sigma + SLOPE * active * (1.0 - sigma)
        gpg = jnp.where(gate_pre < LIMIT, hidden_grad * (linear + 1.0) * slope, 0.0).astype(BF16)
        upg = jnp.where(jnp.abs(up_pre) < LIMIT, hidden_grad * active, 0.0).astype(BF16)
        ga[at_all, :] = gpg
        ua[at_all, :] = upg
        ha[at_all, :] = hidden
        for slab in range(ny):
            c0 = slab * width
            term = nt(gpg, wg[c0 : c0 + width, :]) + nt(upg, wu[c0 : c0 + width, :])
            rt[g, slab] = term.astype(BF16)
        low, high = pl.ds(0, half), pl.ds(half, half)
        remote(rt.at[g, far, low], ra.at[g, 0], ra_send, ra_recv.at[0, g], me, right).start()
        remote(rt.at[g, far, high], ra.at[g, 1], ra_send, ra_recv.at[1, g], me, left).start()
        remote(rt.at[g, right, high], rb.at[g, 0, high], rb_send, rb_recv.at[0, g], me, right).start()
        remote(rt.at[g, left, low], rb.at[g, 1, low], rb_send, rb_recv.at[1, g], me, left).start()
        product = jnp.sum(hidden.astype(F32) * hidden_grad, axis=1, keepdims=True)
        laid = nn(from_src, jnp.where(at_slot, product, 0.0), HIGH)
        for src in range(nj):
            pq[g, src] = laid[src : src + 1, :]
        zs = lax.rem(z - step_of(g) + nz, nz)
        for o in range(nj):
            to = other_j(o)

            def send_products(to=to):
                remote(pq.at[g, to], qin.at[me], q_send, q_recv, zs * nj + to, y).start()

            if o == 0:
                pl.when(g > 0)(send_products)
            else:
                send_products()

    def partly(g):
        low, high = pl.ds(0, half), pl.ds(half, half)
        await_bytes(ra.at[g, 0], ra_recv.at[0, g])
        rc[g, 0] = (ra[g, 0].astype(F32) + rt[g, right, low].astype(F32)).astype(BF16)
        remote(rc.at[g, 0], rb.at[g, 0, low], rb_send, rb_recv.at[0, g], me, right).start()
        await_bytes(ra.at[g, 1], ra_recv.at[1, g])
        rc[g, 1] = (ra[g, 1].astype(F32) + rt[g, left, high].astype(F32)).astype(BF16)
        remote(rc.at[g, 1], rb.at[g, 1, high], rb_send, rb_recv.at[1, g], me, left).start()

    def give_back(g):
        await_bytes(rb.at[g, 0], rb_recv.at[0, g])
        await_bytes(rb.at[g, 1], rb_recv.at[1, g])
        total = rt[g, y].astype(F32) + rb[g, 0].astype(F32) + rb[g, 1].astype(F32)
        done = total.astype(BF16)
        bo[g, :, 0:width] = done[0:main]
        stacked = jnp.concatenate([done[main:rows, q * piece : (q + 1) * piece] for q in range(REST)], axis=0)
        bo[g, :, width:packed] = nn(together, stacked).astype(BF16)
        zs = lax.rem(z - step_of(g) + nz, nz)
        for o in range(nj):
            to = other_j(o)

            def send_rows(to=to):
                remote(bo.at[g, tile(to), :], bk.at[tile(me), :], back_send, back_recv, zs * nj + to, y).start()

            if o == 0:
                pl.when(g > 0)(send_rows)
            else:
                send_rows()

    def step(i, _):
        @pl.when(i == 0)
        def _():
            arrive(3)
            arrive(4)
            forward(3)
            forward(4)

        @pl.when(i == 1)
        def _():
            arrive(1)
            arrive(2)

        pl.when(i == 5)(lambda: arrive(7))
        pl.when((i >= 1) & (i < groups + 1))(lambda: partly(i - 1))

        @pl.when(i == 1)
        def _():
            forward(1)
            forward(2)
            arrive(5)
            arrive(6)

        pl.when(i == 2)(lambda: forward(5))
        pl.when(i == 3)(lambda: forward(6))
        pl.when(i == 6)(lambda: forward(7))
        pl.when(i >= 2)(lambda: give_back(i - 2))
        pl.when(i < groups)(lambda: compute(i))
        return 0

    lax.fori_loop(0, groups + 2, step, 0)

    own_copy = pltpu.make_async_copy(bo.at[0, tile(j), :], bk.at[tile(me), :], own_sem)
    own_copy.start()
    qin[me] = pq[0, j]
    await_bytes(qin.at[pl.ds(0, experts - 1)], q_recv)
    remote(qin, qy.at[0], qy_send.at[0], qy_recv.at[0], me, right).start()
    remote(qin, qy.at[1], qy_send.at[1], qy_recv.at[1], me, left).start()
    remote(qin, qy.at[2], qy_send.at[2], qy_recv.at[2], me, far).start()

    block = min(256, xa.shape[1])

    def weight_grads(i, _):
        at = pl.ds(pl.multiple_of(i * block, block), block)
        dwg[at, :] = tn(xa[:, at], ga[...])
        dwu[at, :] = tn(xa[:, at], ua[...])
        dwd[:, at] = tn(ha[...], da[:, at])
        pltpu.make_async_copy(dwg.at[at, :], dwg_hbm.at[at, :], dw_sem.at[0]).start()
        pltpu.make_async_copy(dwu.at[at, :], dwu_hbm.at[at, :], dw_sem.at[1]).start()
        pltpu.make_async_copy(dwd.at[:, at], dwd_hbm.at[:, at], dw_sem.at[2]).start()
        return 0

    lax.fori_loop(0, xa.shape[1] // block, weight_grads, 0)

    for k in range(3):
        await_bytes(qy.at[k], qy_recv.at[k])
        await_bytes(qin, qy_send.at[k])
    q_out[...] = qin[...] + qy[0] + qy[1] + qy[2]

    await_bytes(m.at[0:2], ep_send)
    await_bytes(m.at[0, 0], ep_send)
    await_bytes(m.at[0, 0, :, 0:half_main, :], ep_send)
    await_bytes(m.at[0:2, :, 0], near_send)
    for _ in range(2):
        await_bytes(m.at[0:5, 0], y_send)
        await_bytes(m.at[0:2, 0, 1], y_send)
        await_bytes(m.at[0:5, 0, :, 0:half_main, :], f_send)
        await_bytes(m.at[0:2, 0, 1, 0:half_main, :], f_send)
        await_bytes(ra.at[:, 0], ra_send)
        await_bytes(rb.at[:, 0], rb_send)
    everything = pl.ds(0, (experts - 1) * MAIN)
    await_bytes(bk.at[everything, :], back_send)
    await_bytes(qin.at[pl.ds(0, experts - 1)], q_send)
    own_copy.wait()
    for k, (a, b) in enumerate(((dwg, dwg_hbm), (dwu, dwu_hbm), (dwd, dwd_hbm))):
        pltpu.make_async_copy(a, b, dw_sem.at[k]).wait()
    await_bytes(bk.at[everything, :], back_recv)


def finish_kernel(
    experts, routes_ref, weights_ref, bk_ref, q_ref, a_in, b_in, c_in,
    grad_ref, gate_ref, a_out, b_out, c_out,
    a, b, c, in_sem, out_sem,
):
    parts = 4
    copies = []
    for n, (src, mid, dst) in enumerate(((a_in, a, a_out), (b_in, b, b_out), (c_in, c, c_out))):
        size = src.shape[0] // parts
        for k in range(parts):
            at = pl.ds(k * size, size)
            first = pltpu.make_async_copy(src.at[at, :], mid.at[at, :], in_sem.at[n, k])
            second = pltpu.make_async_copy(mid.at[at, :], dst.at[at, :], out_sem.at[n, k])
            first.start()
            copies.append((first, second))

    routes = routes_ref[...]
    count = routes.shape[1]
    rank = ranks(routes, experts)
    slots = experts * MAIN
    spread = jnp.where(lax.div(iota((experts, slots), 1), MAIN) == iota((experts, slots), 0), 1.0, 0.0).astype(BF16)
    rk = tn(rank.astype(BF16), spread)
    for first, second in copies[: len(copies) // 2]:
        first.wait()
        second.start()
    lane = lax.rem(iota((count, slots), 1), MAIN)
    width = bk_ref.shape[1] * REST // (REST + 1)
    piece = width // REST
    hot = jnp.where(rk == lane.astype(F32) + 1.0, 1.0, 0.0).astype(BF16)
    total = nn(hot, bk_ref[:, 0:width])
    for first, second in copies[len(copies) // 2 :]:
        first.wait()
        second.start()
    late = rk == lax.rem(lane, REST).astype(F32) + (1.0 + MAIN)
    for q in range(REST):
        hot = jnp.where(late & (lax.div(lane, REST) == q), 1.0, 0.0).astype(BF16)
        at = slice(q * piece, (q + 1) * piece)
        grad_ref[:, at] = (total[:, at] + nn(hot, bk_ref[:, width : width + piece])).astype(BF16)
    products = q_ref[...]
    expert = iota((experts, count), 0)
    for k in range(routes.shape[0]):
        mine = routes[k : k + 1, :] == expert
        slot = jnp.sum(jnp.where(mine, rank, 0.0), axis=0, keepdims=True)
        found = tn(products, jnp.where(mine, 1.0, 0.0), HIGH)
        chosen = jnp.where(iota(found.shape, 0).astype(F32) + 1.0 == slot, found, 0.0)
        gate_ref[k : k + 1, :] = jnp.sum(chosen, axis=0, keepdims=True) / weights_ref[k : k + 1, :]
    for first, second in copies:
        second.wait()


def local(nz, nj, ny, tokens, routes, gate_weights, out_grad, w_gate, w_up, w_down):
    count, model = tokens.shape
    units = w_gate.shape[2]
    top = routes.shape[1]
    experts = nz * nj
    width = model // ny
    packed = width * (REST + 1) // REST
    vmem = pl.BlockSpec(memory_space=pltpu.VMEM)
    hbm = pl.BlockSpec(memory_space=pltpu.HBM)
    routes_t, weights_t = routes.T, gate_weights.T

    groups, main, rows = nz, nj * MAIN, nj * (MAIN + REST)
    all_rows = groups * rows
    dma = pltpu.SemaphoreType.DMA
    weight_shapes = (
        jax.ShapeDtypeStruct((model, units), F32),
        jax.ShapeDtypeStruct((model, units), F32),
        jax.ShapeDtypeStruct((units, model), F32),
    )
    back, products, dwg, dwu, dwd = pl.pallas_call(
        functools.partial(exchange_kernel, nz, nj, ny),
        out_shape=(
            jax.ShapeDtypeStruct((experts * MAIN, packed), BF16),
            jax.ShapeDtypeStruct((experts, 1, 128), F32),
            *weight_shapes,
        ),
        in_specs=[vmem, vmem] + [hbm] * 5,
        out_specs=(hbm, vmem, hbm, hbm, hbm),
        scratch_shapes=[
            pltpu.VMEM((count, model), BF16),
            pltpu.VMEM((count, model), BF16),
            pltpu.VMEM((model, units), BF16),
            pltpu.VMEM((model, units), BF16),
            pltpu.VMEM((units, model), BF16),
            pltpu.VMEM((experts, count), F32),
            pltpu.VMEM((experts, count), F32),
            pltpu.VMEM((groups, 2, main, packed), BF16),
            pltpu.VMEM((len(NEAR), ny, main, packed), BF16),
            pltpu.VMEM((ny, 2, main, packed), BF16),
            pltpu.VMEM((groups, ny, 2, main, packed), BF16),
            pltpu.VMEM((all_rows, model), BF16),
            pltpu.VMEM((all_rows, model), BF16),
            pltpu.VMEM((all_rows, units), BF16),
            pltpu.VMEM((all_rows, units), BF16),
            pltpu.VMEM((all_rows, units), BF16),
            pltpu.VMEM((groups, ny, rows, width), BF16),
            pltpu.VMEM((groups, 2, rows // 2, width), BF16),
            pltpu.VMEM((groups, 2, rows, width), BF16),
            pltpu.VMEM((groups, 2, rows // 2, width), BF16),
            pltpu.VMEM((groups, main, packed), BF16),
            pltpu.VMEM((groups, nj, 1, 128), F32),
            pltpu.VMEM((experts, 1, 128), F32),
            pltpu.VMEM((3, experts, 1, 128), F32),
            *(pltpu.VMEM(w.shape, F32) for w in weight_shapes),
            dma((2,)), dma((3,)), dma, dma((3,)),
            dma, dma((groups,)),
            dma, dma((len(NEAR),)),
            dma, dma((2, groups)),
            dma, dma((2, groups)),
            dma, dma((2, groups)),
            dma, dma((2, groups)),
            dma, dma,
            dma, dma,
            dma((3,)), dma((3,)),
        ],
        compiler_params=pltpu.CompilerParams(
            collective_id=0, has_side_effects=True, vmem_limit_bytes=67_043_328
        ),
        name="exchange",
    )(routes_t, weights_t, tokens, out_grad, w_gate[0], w_up[0], w_down[0])

    token_grad, gate_grad, dwg, dwu, dwd = pl.pallas_call(
        functools.partial(finish_kernel, experts),
        out_shape=(
            jax.ShapeDtypeStruct((count, width), BF16),
            jax.ShapeDtypeStruct((top, count), F32),
            *weight_shapes,
        ),
        in_specs=[vmem] * 4 + [hbm] * 3,
        out_specs=(vmem, vmem, hbm, hbm, hbm),
        scratch_shapes=[*(pltpu.VMEM(w.shape, F32) for w in weight_shapes), dma((3, 4)), dma((3, 4))],
        compiler_params=pltpu.CompilerParams(vmem_limit_bytes=67_043_328),
        name="finish",
    )(routes_t, weights_t, back, products.reshape(experts, 128), dwg, dwu, dwd)
    return token_grad, gate_grad.T, dwg[None], dwu[None], dwd[None]


def solution(mesh):
    nj = CHIPS_X * CORES
    nz, ny = mesh.shape["ep"] // nj, mesh.shape["tp"]
    in_specs = (
        P("ep", None),
        P("ep", None),
        P("ep", None),
        P("ep", None),
        P("ep", None, "tp"),
        P("ep", None, "tp"),
        P("ep", "tp", None),
    )
    out_specs = (P("ep", "tp"), P("ep", None), P("ep", None, "tp"), P("ep", None, "tp"), P("ep", "tp", None))
    return jax.shard_map(
        functools.partial(local, nz, nj, ny), mesh=mesh, in_specs=in_specs, out_specs=out_specs, check_vma=False
    )
```

time: 199 us -> 172 us (0.86)
  local copies, waits for them, and re-layouts: 15.2 us -> 0 us
  Pallas kernels: 183 us -> 170 us
    pallas_call x1, Pallas kernels: 179 us -> 162 us  [local(): pl.pallas_call(functools.partial(exchange_kernel, nz, nj, ny), out_shape=...]
    unnamed x20 -> x0, local copies, waits for them, and re-layouts: 15.2 us -> none
    pallas_call x2 -> x1, Pallas kernels: 4.14 us -> 7.91 us  [local(): pl.pallas_call(functools.partial(finish_kernel, experts), out_shape=(jax....]
where the time goes in v2:
time: 172 us; the launch traced here: 170 us
  Pallas kernels  170 us (99%)
    pallas_call x1, Pallas kernels, local(): pl.pallas_call(functools.partial(exchange_kernel, nz, nj, ny), out_shape=...  162 us
    pallas_call x1, Pallas kernels, local(): pl.pallas_call(functools.partial(finish_kernel, experts), out_shape=(jax....  7.91 us

profile of v2, /device:TPU:1, one launch (start us, length us, event | category | flops | bytes accessed | tf_op | source)
XLA Modules:
  0.0 170.4 jit_solution(1335278899571126087)
XLA Ops:
  0.6 161.8 %exchange.1 = (bf16[1024,640]{1,0:T(8,128)(2,1)}, f32[64,1,128]{2,1,0:T(1,128)}, f32[2048,256]{1,0:T(8,128)}, f32[2048,256]{1,0:T(8,128)}, f32[256,2048]{1,0:T(8,128)}) custom-call(s32[4,256]{1,0:T(4,128)} %bitcast.14, f32[4,256]{1,0:T(4,128)} %bitcast.16, bf16[256,2048]{1,0:T(8,128)(2,1)} %tokens.1, bf16[256,2048]{1,0:T(8,128)(2,1)} %grads.1, ...), custom_call_target="tpu_custom_call" | custom-call | tf_op jit(solution)/shard_map/exchange/pallas_call | solution.py:484
  162.4 7.9 %finish.1 = (bf16[256,512]{1,0:T(8,128)(2,1)}, f32[4,256]{1,0:T(4,128)}, f32[2048,256]{1,0:T(8,128)}, f32[2048,256]{1,0:T(8,128)}, f32[256,2048]{1,0:T(8,128)}) custom-call(s32[4,256]{1,0:T(4,128)} %bitcast.15, f32[4,256]{1,0:T(4,128)} %bitcast.17, bf16[1024,640]{1,0:T(8,128)(2,1)} %get-tuple-element.15.bk_ref, f32[64,128]{1,0:T(8,128)} %bitcast.13, ...), custom_call_target="tpu_custom_call" | custom-call | tf_op jit(solution)/shard_map/finish/pallas_call | solution.py:536

commit v3 on v2

--- a/solution.py
+++ b/solution.py
@@ -17,8 +17,8 @@
 REST = 4
 SLOPE = 1.702
 LIMIT = 7.0
-DISTANCE = (0, 2, -2, 1, -1, 3, -3, 4)
-NEAR = (3, 4)
+DISTANCE = (0, 2, -2, 3, -3, 4, 1, -1)
+NEAR = (6, 7)
 
 
 def nt(a, b, precision=None):
@@ -172,7 +172,7 @@
 
     lax.fori_loop(1, groups, pack_own, 0)
     pl.semaphore_wait(barrier, experts - 1 + 3)
-    for g in (3, 4, 1, 2):
+    for g in (6, 7, 1, 2):
         send_own(g)
 
     picks = pickers(0)
@@ -187,7 +187,7 @@
     for slab in range(ny):
         for k in range(2):
             m[0, slab, k, tile(j), :] = s_here[slab, k, tile(j), :]
-    for g in (5, 6):
+    for g in (3, 4, 5):
         send_own(g)
     for n, g in enumerate(NEAR):
         picks = pickers(g)
@@ -199,7 +199,6 @@
             remote(
                 s_near.at[n, :, tile(to), :], m.at[g, :, 0, tile(j), :], near_send, near_recv.at[n], zd * nj + to, y
             ).start()
-    send_own(7)
 
     a, b = iota((main, main), 0), iota((main, main), 1)
     q_of, src_of, j_of = lax.div(a, rest), lax.div(lax.rem(a, rest), REST), lax.rem(a, REST)
@@ -333,46 +332,6 @@
             else:
                 send_rows()
 
-    def step(i, _):
-        @pl.when(i == 0)
-        def _():
-            arrive(3)
-            arrive(4)
-            forward(3)
-            forward(4)
-
-        @pl.when(i == 1)
-        def _():
-            arrive(1)
-            arrive(2)
-
-        pl.when(i == 5)(lambda: arrive(7))
-        pl.when((i >= 1) & (i < groups + 1))(lambda: partly(i - 1))
-
-        @pl.when(i == 1)
-        def _():
-            forward(1)
-            forward(2)
-            arrive(5)
-            arrive(6)
-
-        pl.when(i == 2)(lambda: forward(5))
-        pl.when(i == 3)(lambda: forward(6))
-        pl.when(i == 6)(lambda: forward(7))
-        pl.when(i >= 2)(lambda: give_back(i - 2))
-        pl.when(i < groups)(lambda: compute(i))
-        return 0
-
-    lax.fori_loop(0, groups + 2, step, 0)
-
-    own_copy = pltpu.make_async_copy(bo.at[0, tile(j), :], bk.at[tile(me), :], own_sem)
-    own_copy.start()
-    qin[me] = pq[0, j]
-    await_bytes(qin.at[pl.ds(0, experts - 1)], q_recv)
-    remote(qin, qy.at[0], qy_send.at[0], qy_recv.at[0], me, right).start()
-    remote(qin, qy.at[1], qy_send.at[1], qy_recv.at[1], me, left).start()
-    remote(qin, qy.at[2], qy_send.at[2], qy_recv.at[2], me, far).start()
-
     block = min(256, xa.shape[1])
 
     def weight_grads(i, _):
@@ -385,7 +344,50 @@
         pltpu.make_async_copy(dwd.at[:, at], dwd_hbm.at[:, at], dw_sem.at[2]).start()
         return 0
 
-    lax.fori_loop(0, xa.shape[1] // block, weight_grads, 0)
+    def step(i, _):
+        @pl.when(i == 0)
+        def _():
+            arrive(6)
+            arrive(7)
+            forward(6)
+            forward(7)
+            arrive(1)
+            arrive(2)
+
+        @pl.when(i == 1)
+        def _():
+            forward(1)
+            forward(2)
+            arrive(3)
+            arrive(4)
+
+        pl.when(i == 2)(lambda: forward(3))
+        pl.when(i == 3)(lambda: arrive(5))
+        pl.when(i == 4)(lambda: forward(5))
+        compute(i)
+        pl.when(i == 2)(lambda: forward(4))
+        pl.when(i >= 1)(lambda: partly(i - 1))
+        pl.when(i >= 2)(lambda: give_back(i - 2))
+        return 0
+
+    lax.fori_loop(0, groups, step, 0)
+    blocks = xa.shape[1] // block
+    cuts = (0, blocks * 3 // 8, blocks * 6 // 8, blocks)
+    lax.fori_loop(cuts[0], cuts[1], weight_grads, 0)
+    partly(groups - 1)
+    give_back(groups - 2)
+    lax.fori_loop(cuts[1], cuts[2], weight_grads, 0)
+    give_back(groups - 1)
+
+    own_copy = pltpu.make_async_copy(bo.at[0, tile(j), :], bk.at[tile(me), :], own_sem)
+    own_copy.start()
+    qin[me] = pq[0, j]
+    await_bytes(qin.at[pl.ds(0, experts - 1)], q_recv)
+    remote(qin, qy.at[0], qy_send.at[0], qy_recv.at[0], me, right).start()
+    remote(qin, qy.at[1], qy_send.at[1], qy_recv.at[1], me, left).start()
+    remote(qin, qy.at[2], qy_send.at[2], qy_recv.at[2], me, far).start()
+
+    lax.fori_loop(cuts[2], cuts[3], weight_grads, 0)
 
     for k in range(3):
         await_bytes(qy.at[k], qy_recv.at[k])

time: 172 us -> 151 us (0.88); the launches traced: 170 us -> 151 us
  Pallas kernels: 170 us -> 151 us
    pallas_call x1, Pallas kernels: 162 us -> 143 us  [local(): pl.pallas_call(functools.partial(exchange_kernel, nz, nj, ny), out_shape=...]
where the time goes in v3:
time: 151 us
  Pallas kernels  151 us (100%)
    pallas_call x1, Pallas kernels, local(): pl.pallas_call(functools.partial(exchange_kernel, nz, nj, ny), out_shape=...  143 us
    pallas_call x1, Pallas kernels, local(): pl.pallas_call(functools.partial(finish_kernel, experts), out_shape=(jax....  7.9 us

profile of v3, /device:TPU:1, one launch (start us, length us, event | category | flops | bytes accessed | tf_op | source)
XLA Modules:
  0.0 151.1 jit_solution(10310947931658015913)
XLA Ops:
  0.6 142.6 %exchange.1 = (bf16[1024,640]{1,0:T(8,128)(2,1)}, f32[64,1,128]{2,1,0:T(1,128)}, f32[2048,256]{1,0:T(8,128)}, f32[2048,256]{1,0:T(8,128)}, f32[256,2048]{1,0:T(8,128)}) custom-call(s32[4,256]{1,0:T(4,128)} %bitcast.14, f32[4,256]{1,0:T(4,128)} %bitcast.16, bf16[256,2048]{1,0:T(8,128)(2,1)} %tokens.1, bf16[256,2048]{1,0:T(8,128)(2,1)} %grads.1, ...), custom_call_target="tpu_custom_call" | custom-call | tf_op jit(solution)/shard_map/exchange/pallas_call | solution.py:486
  143.2 7.9 %finish.1 = (bf16[256,512]{1,0:T(8,128)(2,1)}, f32[4,256]{1,0:T(4,128)}, f32[2048,256]{1,0:T(8,128)}, f32[2048,256]{1,0:T(8,128)}, f32[256,2048]{1,0:T(8,128)}) custom-call(s32[4,256]{1,0:T(4,128)} %bitcast.15, f32[4,256]{1,0:T(4,128)} %bitcast.17, bf16[1024,640]{1,0:T(8,128)(2,1)} %get-tuple-element.15.bk_ref, f32[64,128]{1,0:T(8,128)} %bitcast.13, ...), custom_call_target="tpu_custom_call" | custom-call | tf_op jit(solution)/shard_map/finish/pallas_call | solution.py:538

commit v4 on v3

--- a/solution.py
+++ b/solution.py
@@ -15,6 +15,7 @@
 CHIPS_X = 4
 MAIN = 16
 REST = 4
+SPLIT = 384
 SLOPE = 1.702
 LIMIT = 7.0
 DISTANCE = (0, 2, -2, 3, -3, 4, 1, -1)
@@ -51,7 +52,7 @@
     nz, nj, ny,
     routes, weights, tokens, grads, wg_hbm, wu_hbm, wd_hbm,
     bk, q_out, dwg_hbm, dwu_hbm, dwd_hbm,
-    x_in, dy_in, wg, wu, wd, rank, weight, s, s_near, s_here, m, xa, da, ga, ua, ha, rt, ra, rb, rc, bo, pq, qin, qy,
+    x_in, dy_in, wg, wu, wd, rank, weight, s, s_near, s_edge, s_here, m, xa, da, ga, ua, ha, rt, ra, rb, rc, bo, pq, qin, qy,
     dwg, dwu, dwd,
     in_sem, w_sem, own_sem, dw_sem,
     ep_send, ep_recv, near_send, near_recv, y_send, y_recv, f_send, f_recv, ra_send, ra_recv, rb_send, rb_recv,
@@ -165,7 +166,7 @@
             to = other_j(o)
             dest = zd * nj + to
             if g in NEAR:
-                src, dst = s.at[g, 1, tile(to), :], m.at[g, y, 1, tile(j), :]
+                src, dst = s.at[g, 1, tile(to), SPLIT:packed], m.at[g, y, 1, tile(j), SPLIT:packed]
             else:
                 src, dst = s.at[g, :, tile(to), :], m.at[g, y, :, tile(j), :]
             remote(src, dst, ep_send, ep_recv.at[g], dest, y).start()
@@ -192,13 +193,18 @@
     for n, g in enumerate(NEAR):
         picks = pickers(g)
         for slab in range(ny):
-            pack(s_near.at[n, slab], x_in[:, slab * width : (slab + 1) * width], picks, False)
+            c0 = slab * width
+            pack(s_near.at[n, slab], x_in[:, c0 : c0 + width], picks, False)
+            hot, scale = picks[0]
+            s_edge[n, slab] = (nn(hot, dy_in[:, c0 : c0 + SPLIT]) * scale).astype(BF16)
         zd = lax.rem(z + step_of(g), nz)
         for o in range(nj):
             to = other_j(o)
-            remote(
-                s_near.at[n, :, tile(to), :], m.at[g, :, 0, tile(j), :], near_send, near_recv.at[n], zd * nj + to, y
-            ).start()
+            dest = zd * nj + to
+            src, dst = s_near.at[n, :, tile(to), :], m.at[g, :, 0, tile(j), :]
+            remote(src, dst, near_send, near_recv.at[0, n], dest, y).start()
+            src, dst = s_edge.at[n, :, tile(to), :], m.at[g, :, 1, tile(j), 0:SPLIT]
+            remote(src, dst, near_send, near_recv.at[1, n], dest, y).start()
 
     a, b = iota((main, main), 0), iota((main, main), 1)
     q_of, src_of, j_of = lax.div(a, rest), lax.div(lax.rem(a, rest), REST), lax.rem(a, REST)
@@ -213,11 +219,11 @@
     from_src = jnp.where(from_src, 1.0, 0.0)
 
     def part(g, slab):
-        return m.at[g, slab, 1] if g in NEAR else m.at[g, slab]
+        return m.at[g, slab, 1, :, SPLIT:packed] if g in NEAR else m.at[g, slab]
 
     def halves(g, slab):
         if g in NEAR:
-            return [m.at[g, slab, 1, pl.ds(h * half_main, half_main), :] for h in range(2)]
+            return [m.at[g, slab, 1, pl.ds(h * half_main, half_main), SPLIT:packed] for h in range(2)]
         return [m.at[g, slab, :, pl.ds(h * half_main, half_main), :] for h in range(2)]
 
     def arrive(g):
@@ -244,7 +250,8 @@
 
             @pl.when(g == near)
             def _(n=n, near=near):
-                await_bytes(m.at[near, :, 0], near_recv.at[n])
+                await_bytes(m.at[near, :, 0], near_recv.at[0, n])
+                await_bytes(m.at[near, :, 1, :, 0:SPLIT], near_recv.at[1, n])
                 for h in range(2):
                     await_bytes(halves(near, far)[h], f_recv.at[h, near])
 
@@ -395,14 +402,15 @@
     q_out[...] = qin[...] + qy[0] + qy[1] + qy[2]
 
     await_bytes(m.at[0:2], ep_send)
-    await_bytes(m.at[0, 0], ep_send)
     await_bytes(m.at[0, 0, :, 0:half_main, :], ep_send)
+    await_bytes(m.at[0, 0:2, 0, :, SPLIT:packed], ep_send)
     await_bytes(m.at[0:2, :, 0], near_send)
+    await_bytes(m.at[0:2, :, 1, :, 0:SPLIT], near_send)
     for _ in range(2):
         await_bytes(m.at[0:5, 0], y_send)
-        await_bytes(m.at[0:2, 0, 1], y_send)
+        await_bytes(m.at[0:2, 0, 1, :, SPLIT:packed], y_send)
         await_bytes(m.at[0:5, 0, :, 0:half_main, :], f_send)
-        await_bytes(m.at[0:2, 0, 1, 0:half_main, :], f_send)
+        await_bytes(m.at[0:2, 0, 1, 0:half_main, SPLIT:packed], f_send)
         await_bytes(ra.at[:, 0], ra_send)
         await_bytes(rb.at[:, 0], rb_send)
     everything = pl.ds(0, (experts - 1) * MAIN)
@@ -415,11 +423,15 @@
 
 
 def finish_kernel(
-    experts, routes_ref, weights_ref, bk_ref, q_ref, a_in, b_in, c_in,
+    experts, routes_ref, weights_ref, bk_in, q_in, a_in, b_in, c_in,
     grad_ref, gate_ref, a_out, b_out, c_out,
-    a, b, c, in_sem, out_sem,
+    bk, q, a, b, c, first_sem, in_sem, out_sem,
 ):
     parts = 4
+    load_bk = pltpu.make_async_copy(bk_in, bk, first_sem.at[0])
+    load_q = pltpu.make_async_copy(q_in, q, first_sem.at[1])
+    load_q.start()
+    load_bk.start()
     copies = []
     for n, (src, mid, dst) in enumerate(((a_in, a, a_out), (b_in, b, b_out), (c_in, c, c_out))):
         size = src.shape[0] // parts
@@ -430,29 +442,19 @@
             first.start()
             copies.append((first, second))
 
+    def pass_on(some):
+        for first, second in some:
+            first.wait()
+            second.start()
+
     routes = routes_ref[...]
     count = routes.shape[1]
     rank = ranks(routes, experts)
     slots = experts * MAIN
     spread = jnp.where(lax.div(iota((experts, slots), 1), MAIN) == iota((experts, slots), 0), 1.0, 0.0).astype(BF16)
     rk = tn(rank.astype(BF16), spread)
-    for first, second in copies[: len(copies) // 2]:
-        first.wait()
-        second.start()
-    lane = lax.rem(iota((count, slots), 1), MAIN)
-    width = bk_ref.shape[1] * REST // (REST + 1)
-    piece = width // REST
-    hot = jnp.where(rk == lane.astype(F32) + 1.0, 1.0, 0.0).astype(BF16)
-    total = nn(hot, bk_ref[:, 0:width])
-    for first, second in copies[len(copies) // 2 :]:
-        first.wait()
-        second.start()
-    late = rk == lax.rem(lane, REST).astype(F32) + (1.0 + MAIN)
-    for q in range(REST):
-        hot = jnp.where(late & (lax.div(lane, REST) == q), 1.0, 0.0).astype(BF16)
-        at = slice(q * piece, (q + 1) * piece)
-        grad_ref[:, at] = (total[:, at] + nn(hot, bk_ref[:, width : width + piece])).astype(BF16)
-    products = q_ref[...]
+    load_q.wait()
+    products = q[...]
     expert = iota((experts, count), 0)
     for k in range(routes.shape[0]):
         mine = routes[k : k + 1, :] == expert
@@ -460,7 +462,21 @@
         found = tn(products, jnp.where(mine, 1.0, 0.0), HIGH)
         chosen = jnp.where(iota(found.shape, 0).astype(F32) + 1.0 == slot, found, 0.0)
         gate_ref[k : k + 1, :] = jnp.sum(chosen, axis=0, keepdims=True) / weights_ref[k : k + 1, :]
-    for first, second in copies:
+    pass_on(copies[:5])
+    lane = lax.rem(iota((count, slots), 1), MAIN)
+    width = bk.shape[1] * REST // (REST + 1)
+    piece = width // REST
+    hot = jnp.where(rk == lane.astype(F32) + 1.0, 1.0, 0.0).astype(BF16)
+    load_bk.wait()
+    total = nn(hot, bk[:, 0:width])
+    pass_on(copies[5:9])
+    late = rk == lax.rem(lane, REST).astype(F32) + (1.0 + MAIN)
+    for n in range(REST):
+        hot = jnp.where(late & (lax.div(lane, REST) == n), 1.0, 0.0).astype(BF16)
+        at = slice(n * piece, (n + 1) * piece)
+        grad_ref[:, at] = (total[:, at] + nn(hot, bk[:, width : width + piece])).astype(BF16)
+    pass_on(copies[9:])
+    for _, second in copies:
         second.wait()
 
 
@@ -502,6 +518,7 @@
             pltpu.VMEM((experts, count), F32),
             pltpu.VMEM((groups, 2, main, packed), BF16),
             pltpu.VMEM((len(NEAR), ny, main, packed), BF16),
+            pltpu.VMEM((len(NEAR), ny, main, SPLIT), BF16),
             pltpu.VMEM((ny, 2, main, packed), BF16),
             pltpu.VMEM((groups, ny, 2, main, packed), BF16),
             pltpu.VMEM((all_rows, model), BF16),
@@ -520,7 +537,7 @@
             *(pltpu.VMEM(w.shape, F32) for w in weight_shapes),
             dma((2,)), dma((3,)), dma, dma((3,)),
             dma, dma((groups,)),
-            dma, dma((len(NEAR),)),
+            dma, dma((2, len(NEAR))),
             dma, dma((2, groups)),
             dma, dma((2, groups)),
             dma, dma((2, groups)),
@@ -542,9 +559,14 @@
             jax.ShapeDtypeStruct((top, count), F32),
             *weight_shapes,
         ),
-        in_specs=[vmem] * 4 + [hbm] * 3,
+        in_specs=[vmem] * 2 + [hbm] * 5,
         out_specs=(vmem, vmem, hbm, hbm, hbm),
-        scratch_shapes=[*(pltpu.VMEM(w.shape, F32) for w in weight_shapes), dma((3, 4)), dma((3, 4))],
+        scratch_shapes=[
+            pltpu.VMEM((experts * MAIN, packed), BF16),
+            pltpu.VMEM((experts, 128), F32),
+            *(pltpu.VMEM(w.shape, F32) for w in weight_shapes),
+            dma((2,)), dma((3, 4)), dma((3, 4)),
+        ],
         compiler_params=pltpu.CompilerParams(vmem_limit_bytes=67_043_328),
         name="finish",
     )(routes_t, weights_t, back, products.reshape(experts, 128), dwg, dwu, dwd)

time: 151 us -> 148 us (0.980)
  Pallas kernels: 151 us -> 148 us
    pallas_call x1, Pallas kernels: 143 us -> 140 us  [local(): pl.pallas_call(functools.partial(exchange_kernel, nz, nj, ny), out_shape=...]
where the time goes in v4:
time: 148 us
  Pallas kernels  148 us (100%)
    pallas_call x1, Pallas kernels, local(): pl.pallas_call(functools.partial(exchange_kernel, nz, nj, ny), out_shape=...  140 us
    pallas_call x1, Pallas kernels, local(): pl.pallas_call(functools.partial(finish_kernel, experts), out_shape=(jax....  7.27 us

profile of v4, /device:TPU:1, one launch (start us, length us, event | category | flops | bytes accessed | tf_op | source)
XLA Modules:
  0.0 148.2 jit_solution(3640374130192212306)
XLA Ops:
  0.6 140.3 %exchange.1 = (bf16[1024,640]{1,0:T(8,128)(2,1)}, f32[64,1,128]{2,1,0:T(1,128)}, f32[2048,256]{1,0:T(8,128)}, f32[2048,256]{1,0:T(8,128)}, f32[256,2048]{1,0:T(8,128)}) custom-call(s32[4,256]{1,0:T(4,128)} %bitcast.14, f32[4,256]{1,0:T(4,128)} %bitcast.16, bf16[256,2048]{1,0:T(8,128)(2,1)} %tokens.1, bf16[256,2048]{1,0:T(8,128)(2,1)} %grads.1, ...), custom_call_target="tpu_custom_call" | custom-call | tf_op jit(solution)/shard_map/exchange/pallas_call | solution.py:502
  141.0 7.3 %finish.1 = (bf16[256,512]{1,0:T(8,128)(2,1)}, f32[4,256]{1,0:T(4,128)}, f32[2048,256]{1,0:T(8,128)}, f32[2048,256]{1,0:T(8,128)}, f32[256,2048]{1,0:T(8,128)}) custom-call(s32[4,256]{1,0:T(4,128)} %bitcast.15, f32[4,256]{1,0:T(4,128)} %bitcast.17, bf16[1024,640]{1,0:T(8,128)(2,1)} %get-tuple-element.15.bk_in, f32[64,128]{1,0:T(8,128)} %bitcast.13, ...), custom_call_target="tpu_custom_call" | custom-call | tf_op jit(solution)/shard_map/finish/pallas_call | solution.py:555

commit v5 on v4

--- a/solution.py
+++ b/solution.py
@@ -427,7 +427,7 @@
     grad_ref, gate_ref, a_out, b_out, c_out,
     bk, q, a, b, c, first_sem, in_sem, out_sem,
 ):
-    parts = 4
+    parts = in_sem.shape[1]
     load_bk = pltpu.make_async_copy(bk_in, bk, first_sem.at[0])
     load_q = pltpu.make_async_copy(q_in, q, first_sem.at[1])
     load_q.start()
@@ -453,6 +453,7 @@
     slots = experts * MAIN
     spread = jnp.where(lax.div(iota((experts, slots), 1), MAIN) == iota((experts, slots), 0), 1.0, 0.0).astype(BF16)
     rk = tn(rank.astype(BF16), spread)
+    pass_on(copies[:4])
     load_q.wait()
     products = q[...]
     expert = iota((experts, count), 0)
@@ -462,20 +463,20 @@
         found = tn(products, jnp.where(mine, 1.0, 0.0), HIGH)
         chosen = jnp.where(iota(found.shape, 0).astype(F32) + 1.0 == slot, found, 0.0)
         gate_ref[k : k + 1, :] = jnp.sum(chosen, axis=0, keepdims=True) / weights_ref[k : k + 1, :]
-    pass_on(copies[:5])
+    pass_on(copies[4:12])
     lane = lax.rem(iota((count, slots), 1), MAIN)
     width = bk.shape[1] * REST // (REST + 1)
     piece = width // REST
     hot = jnp.where(rk == lane.astype(F32) + 1.0, 1.0, 0.0).astype(BF16)
     load_bk.wait()
     total = nn(hot, bk[:, 0:width])
-    pass_on(copies[5:9])
+    pass_on(copies[12:18])
     late = rk == lax.rem(lane, REST).astype(F32) + (1.0 + MAIN)
     for n in range(REST):
         hot = jnp.where(late & (lax.div(lane, REST) == n), 1.0, 0.0).astype(BF16)
         at = slice(n * piece, (n + 1) * piece)
         grad_ref[:, at] = (total[:, at] + nn(hot, bk[:, width : width + piece])).astype(BF16)
-    pass_on(copies[9:])
+    pass_on(copies[18:])
     for _, second in copies:
         second.wait()
 
@@ -565,7 +566,7 @@
             pltpu.VMEM((experts * MAIN, packed), BF16),
             pltpu.VMEM((experts, 128), F32),
             *(pltpu.VMEM(w.shape, F32) for w in weight_shapes),
-            dma((2,)), dma((3, 4)), dma((3, 4)),
+            dma((2,)), dma((3, 8)), dma((3, 8)),
         ],
         compiler_params=pltpu.CompilerParams(vmem_limit_bytes=67_043_328),
         name="finish",

time: 148 us -> 149 us (level)
  no operation moved by 1% of the time
where the time goes in v5:
time: 149 us
  Pallas kernels  148 us (99%)
    pallas_call x1, Pallas kernels, local(): pl.pallas_call(functools.partial(exchange_kernel, nz, nj, ny), out_shape=...  140 us
    pallas_call x1, Pallas kernels, local(): pl.pallas_call(functools.partial(finish_kernel, experts), out_shape=(jax....  7.68 us

profile of v5, /device:TPU:1, one launch (start us, length us, event | category | flops | bytes accessed | tf_op | source)
XLA Modules:
  0.0 148.6 jit_solution(4037071966821020870)
XLA Ops:
  0.6 140.3 %exchange.1 = (bf16[1024,640]{1,0:T(8,128)(2,1)}, f32[64,1,128]{2,1,0:T(1,128)}, f32[2048,256]{1,0:T(8,128)}, f32[2048,256]{1,0:T(8,128)}, f32[256,2048]{1,0:T(8,128)}) custom-call(s32[4,256]{1,0:T(4,128)} %bitcast.14, f32[4,256]{1,0:T(4,128)} %bitcast.16, bf16[256,2048]{1,0:T(8,128)(2,1)} %tokens.1, bf16[256,2048]{1,0:T(8,128)(2,1)} %grads.1, ...), custom_call_target="tpu_custom_call" | custom-call | tf_op jit(solution)/shard_map/exchange/pallas_call | solution.py:503
  141.0 7.7 %finish.1 = (bf16[256,512]{1,0:T(8,128)(2,1)}, f32[4,256]{1,0:T(4,128)}, f32[2048,256]{1,0:T(8,128)}, f32[2048,256]{1,0:T(8,128)}, f32[256,2048]{1,0:T(8,128)}) custom-call(s32[4,256]{1,0:T(4,128)} %bitcast.15, f32[4,256]{1,0:T(4,128)} %bitcast.17, bf16[1024,640]{1,0:T(8,128)(2,1)} %get-tuple-element.15.bk_in, f32[64,128]{1,0:T(8,128)} %bitcast.13, ...), custom_call_target="tpu_custom_call" | custom-call | tf_op jit(solution)/shard_map/finish/pallas_call | solution.py:556
